TPU v7x, 32 devices: a whole 2x2x4 slice. The times are simulated.
32 devices in a mesh: ep: 8 (over z, core), tp: 4 (over y, x).
Axes of the slice: x: 2, y: 2, z: 4, core: 2. Of those that a mesh axis runs over, the one named last changes fastest.
Arguments:
- stream: bfloat16 [128, 4096], P('ep'), may hold values from -6 to 6
- previous_state: float32 [128, 128, 4096], P('ep', None, 'tp'), may hold values from -6 to 6
- mixer_norm_gain: float32 [4096], replicated, may hold values from 0.1 to 1.9
- query_matrix: bfloat16 [4096, 2048], P('ep'), may hold values from -0.09375 to 0.09375
- key_matrix: bfloat16 [4096, 2048], P('ep'), may hold values from -0.09375 to 0.09375
- value_matrix: bfloat16 [4096, 4096], P('ep', 'tp'), may hold values from -0.09375 to 0.09375
- output_gate_weight: bfloat16 [4096, 4096], P('ep', 'tp'), may hold values from -0.09375 to 0.09375
- decay_lower_factor: bfloat16 [4096, 64], replicated, may hold values from -0.09375 to 0.09375
- decay_upper_factor: bfloat16 [64, 2048], replicated, may hold values from -3 to 3
- forgetting_boost: float32 [128, 2048], P('ep'), may hold values from 0.02 to 1.5
- head_norm_gain: float32 [256], replicated, may hold values from 0.1 to 1.9
- output_matrix: bfloat16 [4096, 4096], P('tp'), may hold values from -0.1875 to 0.1875
- mixture_norm_gain: float32 [4096], replicated, may hold values from 0.1 to 1.9
- expert_gate_weight: bfloat16 [8, 1024, 4096], P('ep', 'tp'), may hold values from -0.09375 to 0.09375
- expert_up_weight: bfloat16 [8, 1024, 4096], P('ep', 'tp'), may hold values from -0.09375 to 0.09375
- expert_down_weight: bfloat16 [8, 1024, 4096], P('ep', None, 'tp'), may hold values from -0.375 to 0.375
- expert_index_table: int32 [128, 2], P('ep'), may hold values from 0 to 7, as said below
- expert_scores_within: float32 [128, 2], P('ep'), may hold values from -6 to 6
- group_probability: float32 [128], P('ep'), may hold values from 0.3 to 1
Outputs:
- new_stream: bfloat16 [128, 4096], P('ep', 'tp')
- new_state: float32 [128, 128, 4096], P('ep', None, 'tp')
Inputs may be any that keep to these rules, and one draw needn't show every extreme that they name: `expert_index_table`: the 2 experts of a sequence are distinct and lie in one group of 2 consecutive experts. Among the 16 sequences of one index of ep (aligned blocks of rows), each expert is named at most 8 times, and in every block some experts are named exactly 8 times.
All inputs are finite; a program needn't handle non-finite values.
Results may differ from a plain program's by a relative error of at most 0.02.
Values may be sent and summed in bfloat16 or wider, within the bound.
No kernel may reach another device: no remote copies, remote signals or barrier semaphores. Data moves between devices by JAX's collectives and lax.ppermute only.
A program may use at most 128 MiB of HBM per device.

v0:
```python
import jax
import jax.numpy as jnp
from jax import lax
from jax.sharding import PartitionSpec as P

HEAD_TOTAL = 16
KEY_CHANNELS = 128
DV = 256


epsilon = 1e-06
forgetting_softness = 16.0


def rms_scaled(values, gain_vec):
    floats = values.astype(jnp.float32)
    scaled = floats * lax.rsqrt(jnp.mean(floats * floats, axis=-1, keepdims=True) + epsilon)
    return (scaled * gain_vec).astype(jnp.bfloat16)


def on_device(
    stream,
    previous_state,
    mixer_norm_gain,
    query_matrix,
    key_matrix,
    value_matrix,
    output_gate_weight,
    decay_lower_factor,
    decay_upper_factor,
    forgetting_boost,
    head_norm_gain,
    output_matrix,
    mixture_norm_gain,
    expert_gate_weight,
    expert_up_weight,
    expert_down_weight,
    expert_index_table,
    expert_scores_within,
    group_probability,
):
    seq_count, model_width = stream.shape
    value_local = previous_state.shape[2]
    head_count = max(1, value_local // DV)
    head_width = min(value_local, DV)
    tp_index = lax.axis_index("tp")
    leading_head = tp_index * value_local // DV
    value_start = tp_index * value_local % DV
    key_column_span = head_count * KEY_CHANNELS
    normed = rms_scaled(stream, mixer_norm_gain)
    own_query = lax.dynamic_slice_in_dim(
        query_matrix, leading_head * KEY_CHANNELS, key_column_span, 1
    )
    own_key = lax.dynamic_slice_in_dim(key_matrix, leading_head * KEY_CHANNELS, key_column_span, 1)
    spread = lax.all_to_all(normed, "ep", split_axis=1, concat_axis=0, tiled=True)
    joined = jnp.concatenate([own_query, own_key, value_matrix, output_gate_weight], axis=1)
    summed = lax.psum_scatter(
        jnp.dot(spread, joined, preferred_element_type=jnp.float32),
        "ep",
        scatter_dimension=0,
        tiled=True,
    )
    query_sum = summed[:, :key_column_span]
    key_sum = summed[:, key_column_span : 2 * key_column_span]
    value_sum = summed[:, 2 * key_column_span : 2 * key_column_span + value_local]
    gate_sum = summed[:, 2 * key_column_span + value_local :]
    queries = (query_sum * KEY_CHANNELS ** (-0.5)).astype(jnp.bfloat16)
    key_rows = key_sum.astype(jnp.bfloat16)
    value_rows = value_sum.astype(jnp.bfloat16)
    gate_rows = gate_sum.astype(jnp.bfloat16)
    low_rank = jnp.dot(normed, decay_lower_factor, preferred_element_type=jnp.float32).astype(
        jnp.bfloat16
    )
    local_expand_matrix = lax.dynamic_slice_in_dim(
        decay_upper_factor, leading_head * KEY_CHANNELS, key_column_span, 1
    )
    forgetting_logit = jnp.dot(low_rank, local_expand_matrix, preferred_element_type=jnp.float32)
    request_boost = lax.dynamic_slice_in_dim(
        forgetting_boost, leading_head * KEY_CHANNELS, key_column_span, 1
    )
    forgetting_lograte = jax.nn.log_sigmoid(forgetting_logit) / forgetting_softness - request_boost
    factor = (
        jnp.exp(forgetting_lograte)
        .reshape(seq_count, head_count, KEY_CHANNELS)
        .transpose(0, 2, 1)[..., None]
    )
    state_four = previous_state.reshape(seq_count, KEY_CHANNELS, head_count, head_width)
    key_part = (
        key_rows.astype(jnp.float32)
        .reshape(seq_count, head_count, KEY_CHANNELS)
        .transpose(0, 2, 1)[..., None]
    )
    value_part = value_rows.astype(jnp.float32).reshape(seq_count, 1, head_count, head_width)
    updated = factor * state_four + key_part * value_part
    query_part = (
        queries.astype(jnp.float32).reshape(seq_count, head_count, KEY_CHANNELS).transpose(0, 2, 1)
    )
    readout = jnp.einsum("skh,skhv->shv", query_part, updated, precision=lax.Precision.HIGHEST)
    square_sums = jnp.sum(readout * readout, axis=-1)
    norm_table = lax.dynamic_update_slice(
        jnp.zeros((seq_count, HEAD_TOTAL), jnp.float32), square_sums, (jnp.int32(0), leading_head)
    )
    totals = lax.psum(norm_table, "tp")
    own_totals = lax.dynamic_slice_in_dim(totals, leading_head, head_count, 1)
    mean_sq = own_totals[..., None] / DV
    own_gain = lax.dynamic_slice_in_dim(head_norm_gain, value_start, head_width, 0)
    gate_part = jax.nn.silu(
        gate_rows.astype(jnp.float32).reshape(seq_count, head_count, head_width)
    )
    gated_rows = (
        (readout * lax.rsqrt(mean_sq + epsilon) * own_gain * gate_part)
        .reshape(seq_count, value_local)
        .astype(jnp.bfloat16)
    )
    partial_out = jnp.dot(gated_rows, output_matrix, preferred_element_type=jnp.float32)
    mixer_sum = lax.psum(partial_out.astype(jnp.bfloat16), "tp").astype(jnp.float32)
    blended_tokens = (stream.astype(jnp.float32) + mixer_sum).astype(jnp.bfloat16)
    normed_two = rms_scaled(blended_tokens, mixture_norm_gain)
    ep_count = lax.axis_size("ep")
    local_experts = expert_gate_weight.shape[0]
    experts_all = ep_count * local_experts
    route_count = expert_index_table.shape[1]
    capacity = 2 * seq_count * route_count // experts_all
    slot_count = experts_all * capacity
    flat_ids = expert_index_table.reshape(seq_count * route_count)
    one_hot = (flat_ids[:, None] == jnp.arange(experts_all, dtype=jnp.int32)[None, :]).astype(
        jnp.int32
    )
    rank_in = jnp.sum(one_hot * (jnp.cumsum(one_hot, axis=0) - 1), axis=1)
    place_lookup = flat_ids * capacity + rank_in
    placing = (place_lookup[:, None] == jnp.arange(slot_count, dtype=jnp.int32)[None, :]).astype(
        jnp.float32
    )
    placing = placing.reshape(seq_count, route_count, slot_count)
    logit_exp = jnp.exp(expert_scores_within)
    weights = logit_exp / jnp.sum(logit_exp, axis=-1, keepdims=True) * group_probability[:, None]
    combine = jnp.einsum("sk,skc->sc", weights, placing, precision=lax.Precision.HIGHEST)
    dispatch = jnp.sum(placing, axis=1).astype(jnp.bfloat16)
    outgoing = jnp.einsum("sc,sd->cd", dispatch, normed_two, preferred_element_type=jnp.float32)
    outgoing = outgoing.astype(jnp.bfloat16).reshape(experts_all, capacity, model_width)
    width_local = expert_down_weight.shape[2]
    arrived = lax.all_to_all(outgoing, "ep", split_axis=0, concat_axis=0, tiled=True)
    held_slots = arrived.shape[1]
    grouped = arrived.reshape(ep_count, local_experts, held_slots, model_width)
    gate_pre = jnp.einsum(
        "sxcd,xfd->sxcf", grouped, expert_gate_weight, preferred_element_type=jnp.float32
    )
    up_pre = jnp.einsum(
        "sxcd,xfd->sxcf", grouped, expert_up_weight, preferred_element_type=jnp.float32
    )
    hidden = (jax.nn.silu(gate_pre) * up_pre).astype(jnp.bfloat16)
    outputs = jnp.einsum(
        "sxcf,xfd->sxcd",
        lax.all_gather(hidden, "tp", axis=3, tiled=True),
        expert_down_weight,
        preferred_element_type=jnp.float32,
    )
    ready_rows = outputs.astype(jnp.bfloat16).reshape(
        ep_count * local_experts, held_slots, width_local
    )
    returned = lax.all_to_all(ready_rows, "ep", split_axis=0, concat_axis=0, tiled=True)
    mixture = jnp.dot(
        combine,
        returned.reshape(slot_count, width_local).astype(jnp.float32),
        precision=lax.Precision.HIGHEST,
    )
    own_mixed = lax.dynamic_slice_in_dim(blended_tokens, tp_index * width_local, width_local, 1)
    new_stream = (own_mixed.astype(jnp.float32) + mixture).astype(jnp.bfloat16)
    return (new_stream, updated.reshape(seq_count, KEY_CHANNELS, value_local))


def solution(mesh):
    placed = (
        P("ep", None),
        P("ep", None, "tp"),
        P(),
        P("ep", None),
        P("ep", None),
        P("ep", "tp"),
        P("ep", "tp"),
        P(),
        P(),
        P("ep", None),
        P(),
        P("tp", None),
        P(),
        P("ep", "tp", None),
        P("ep", "tp", None),
        P("ep", None, "tp"),
        P("ep", None),
        P("ep", None),
        P("ep"),
    )
    return jax.shard_map(
        on_device,
        mesh=mesh,
        in_specs=placed,
        out_specs=(P("ep", "tp"), P("ep", None, "tp")),
        check_vma=False,
    )
```

profile of v0, /device:TPU:0, one launch (start us, length us, event | category | flops | bytes accessed | tf_op | source)
XLA Modules:
  0.0 207.3 jit_solution(5548687518825373681)
XLA Ops:
  7.2 1.2 fusion.36
  8.4 1.0 fusion.38
  9.4 0.7 copy.61
  10.1 6.4 %all-to-all-start = ((bf16[16,8,512]{2,0,1:T(8,128)(2,1)}), bf16[16,8,512]{2,0,1:T(8,128)(2,1)S(1)}, u32[]{:S(2)}, u32[]{:S(2)}) async-start(bf16[16,8,512]{2,0,1:T(8,128)(2,1)} %bitcast.84), calls=%async_computation | async-start | bytes 262144 | tf_op jit(solution)/shard_map/all_to_all | solution.py:55
  16.5 1.3 constant_dynamic-slice_fusion
  17.8 5.4 %all-to-all-done = bf16[16,8,512]{2,0,1:T(8,128)(2,1)S(1)} async-done(((bf16[16,8,512]{2,0,1:T(8,128)(2,1)}), bf16[16,8,512]{2,0,1:T(8,128)(2,1)S(1)}, u32[]{:S(2)}, u32[]{:S(2)}) %all-to-all-start) | async-done | bytes 131104 | tf_op jit(solution)/shard_map/all_to_all | solution.py:55
  23.2 3.3 %fusion.3 = f32[128,3072]{1,0:T(8,128)} fusion(bf16[128,512]{1,0:T(8,128)(2,1)S(1)} %bitcast.90, bf16[512,1024]{1,0:T(8,128)(2,1)} %param.25, bf16[512,1024]{1,0:T(8,128)(2,1)} %param.24, bf16[512,512]{1,0:T(8,128)(2,1)S(1)} %get-tuple-element.6, bf16[512,512]{1,0:T(8,128)(2,1)S(1)} %get-tuple-element.7), kind=kOutput, calls=%fused_computation.7 | convolution fusion | flops 415236096 | bytes 4849664 | tf_op jit(solution)/shard_map/dot_general | solution.py:58
  27.2 10.6 %reshape.119 = f32[16,128,4,256]{3,2,1,0:T(4,128)} reshape(f32[16,128,1024]{2,1,0:T(8,128)} %param.20) | data formatting | bytes 16777216 | tf_op jit(solution)/shard_map/reshape | solution.py:87
  37.8 1.3 fusion.53
  39.5 20.4 %reduce-scatter.2.cloned.1.call-done = f32[16,3072]{1,0:T(8,128)} async-done(((f32[128,3072]{1,0:T(8,128)}), f32[16,3072]{1,0:T(8,128)}) %reduce-scatter.2.cloned.1.call-update) | async-done | bytes 196624 | tf_op jit(solution)/shard_map/reduce_scatter | solution.py:57
  59.9 0.9 convert.8
  61.0 1.4 copy.41
  62.4 0.8 fusion.54
  63.2 6.4 %multiply_add_fusion.1 = f32[16,128,4,256]{3,2,1,0:T(4,128)S(1)} fusion(f32[16,128,4,256]{3,2,1,0:T(4,128)} %reshape.119, f32[16,4,256]{2,1,0:T(4,128)S(1)} %mul.156, f32[16,128,4]{2,1,0:T(8,128)} %copy.41, f32[16,128,4]{2,1,0:T(8,128)S(1)} %copy.40), kind=kLoop, calls=%fused_computation.3 | loop fusion | flops 6291456 | bytes 16908288 | tf_op jit(solution)/shard_map/add | solution.py:94
  69.6 3.4 %fusion = f32[16,4,1,256]{3,2,1,0:T(1,128)S(1)} fusion(f32[16,128,4,256]{3,2,1,0:T(4,128)S(1)} %multiply_add_fusion.1, bf16[16,128,4,1]{1,2,0,3:T(4,128)(2,1)S(1)} %bitcast.87), kind=kOutput, calls=%fused_computation | convolution fusion | flops 25165824 | bytes 8470528 | tf_op jit(solution)/shard_map/skh,skhv->shv/dot_general | solution.py:98
  73.4 10.2 %psum.14 = f32[16,16]{1,0:T(8,128)S(1)} all-reduce(f32[16,16]{1,0:T(8,128)S(1)} %dynamic_update_slice.3), channel_id=1, replica_groups=mesh['ep'=8,'tp'=4] {'tp'}, use_global_device_ids=true, to_apply=%region_3.4 | all-reduce | flops 256 | bytes 2048 | tf_op jit(solution)/shard_map/psum | solution.py:103
  83.9 5.3 %convolution_convert_fusion.1 = bf16[16,4096]{1,0:T(8,128)(2,1)} fusion(bf16[16,1024]{1,0:T(8,128)(2,1)S(1)} %bitcast.86, bf16[1024,4096]{1,0:T(8,128)(2,1)} %param.30), kind=kOutput, calls=%fused_computation.6 | convolution fusion | flops 134283264 | bytes 8552448 | tf_op jit(solution)/shard_map/dot_general | solution.py:115
  89.3 38.6 %all-reduce.2.cloned.1.call-done = bf16[16,4096]{1,0:T(8,128)(2,1)} async-done(((bf16[16,4096]{1,0:T(8,128)(2,1)}), bf16[16,4096]{1,0:T(8,128)(2,1)}) %all-reduce.2.cloned.1.call-update) | async-done | bytes 131088 | tf_op jit(solution)/shard_map/psum | solution.py:116
  127.9 1.1 fusion.33
  129.0 1.2 fusion.2
  130.1 4.6 %all-to-all-start.1 = ((bf16[8,8,4096]{2,1,0:T(8,128)(2,1)}), bf16[8,8,4096]{2,1,0:T(8,128)(2,1)}, u32[]{:S(2)}, u32[]{:S(2)}) async-start(bf16[8,8,4096]{2,1,0:T(8,128)(2,1)} %fusion.2), calls=%async_computation.2 | async-start | bytes 1048576 | tf_op jit(solution)/shard_map/all_to_all | solution.py:142
  134.8 4.5 %mul.153 = f32[16,128,4,256]{3,2,1,0:T(4,128)} broadcast(f32[16,128,4]{2,1,0:T(8,128)S(1)} %copy.40), dimensions={0,1,2} | broadcast | bytes 8421376 | tf_op jit(solution)/shard_map/mul | solution.py:94
  139.4 10.8 %mul.178 = f32[16,128,1024]{2,1,0:T(8,128)} reshape(f32[16,128,4,256]{3,2,1,0:T(4,128)} %mul.153) | data formatting | bytes 16777216 | tf_op jit(solution)/shard_map/mul | solution.py:94
  150.5 4.6 %mul.155 = f32[16,128,4,256]{3,2,1,0:T(4,128)} broadcast(f32[16,128,4]{2,1,0:T(8,128)S(1)} %copy-done.1), dimensions={0,1,2} | broadcast | bytes 8421376 | tf_op jit(solution)/shard_map/mul | solution.py:94
  155.0 10.7 %mul.180 = f32[16,128,1024]{2,1,0:T(8,128)} reshape(f32[16,128,4,256]{3,2,1,0:T(4,128)} %mul.155) | data formatting | bytes 16777216 | tf_op jit(solution)/shard_map/mul | solution.py:94
  165.8 2.5 %fusion.20 = f32[8,1,8,256]{3,2,0,1:T(8,128)S(1)} fusion(bf16[8,8,4096]{2,1,0:T(8,128)(2,1)} %all-to-all-done.1, bf16[1,256,4096]{2,1,0:T(8,128)(2,1)} %param.32), kind=kOutput, calls=%fused_computation.23 | convolution fusion | flops 134217728 | bytes 2686976 | tf_op jit(solution)/shard_map/sxcd,xfd->sxcf/dot_general | solution.py:145
  168.3 2.5 %fusion.29 = bf16[8,1,8,256]{3,2,0,1:T(8,128)(2,1)S(1)} fusion(bf16[8,8,4096]{2,1,0:T(8,128)(2,1)} %all-to-all-done.1, bf16[1,256,4096]{2,1,0:T(8,128)(2,1)} %param.33, f32[8,1,8,256]{3,2,0,1:T(8,128)S(1)} %fusion.20), kind=kOutput, calls=%fused_computation.26 | convolution fusion | flops 134316032 | bytes 2719744 | tf_op jit(solution)/shard_map/sxcd,xfd->sxcf/dot_general | solution.py:148
  170.9 8.9 %all_gather.3 = bf16[8,1,8,1024]{3,2,0,1:T(8,128)(2,1)S(1)} all-gather(bf16[8,1,8,256]{3,2,0,1:T(8,128)(2,1)S(1)} %fusion.29), channel_id=1, replica_groups=mesh['ep'=8,'tp'=4] {'tp'}, dimensions={3}, use_global_device_ids=true | all-gather | bytes 163840 | tf_op jit(solution)/shard_map/all_gather | solution.py:154
  179.8 1.1 fusion.17
  180.9 5.1 %all-to-all-start.2 = ((bf16[8,8,1024]{2,1,0:T(8,128)(2,1)}), bf16[8,8,1024]{2,1,0:T(8,128)(2,1)S(1)}, u32[]{:S(2)}, u32[]{:S(2)}) async-start(bf16[8,8,1024]{2,1,0:T(8,128)(2,1)} %fusion.17), calls=%async_computation.3 | async-start | bytes 262144 | tf_op jit(solution)/shard_map/all_to_all | solution.py:161
  186.0 13.6 %multiply_add_fusion = f32[16,128,1024]{2,1,0:T(8,128)} fusion(f32[16,128,1024]{2,1,0:T(8,128)} %mul.180, f32[16,128,1024]{2,1,0:T(8,128)} %mul.178, f32[16,128,1024]{2,1,0:T(8,128)} %param.20, f32[16,1024]{1,0:T(8,128)S(1)} %get-tuple-element.4), kind=kLoop, calls=%fused_computation.2 | loop fusion | flops 6291456 | bytes 33619968 | tf_op jit(solution)/shard_map/add | solution.py:94
  199.6 0.8 fusion.32
  (54 shorter events, 2.3 us)
Async XLA Ops:
  7.2 172.6 %copy-start = (bf16[1,1024,1024]{2,1,0:T(8,128)(2,1)S(1)}, bf16[1,1024,1024]{2,1,0:T(8,128)(2,1)}, u32[]{:S(2)}) copy-start(bf16[1,1024,1024]{2,1,0:T(8,128)(2,1)} %param.34) | copy-start | bytes 6291460
  10.1 13.1 %all-to-all-start = ((bf16[16,8,512]{2,0,1:T(8,128)(2,1)}), bf16[16,8,512]{2,0,1:T(8,128)(2,1)S(1)}, u32[]{:S(2)}, u32[]{:S(2)}) async-start(bf16[16,8,512]{2,0,1:T(8,128)(2,1)} %bitcast.84), calls=%async_computation | async-start | bytes 262144 | tf_op jit(solution)/shard_map/all_to_all | solution.py:55
  16.4 43.5 %reduce-scatter.2.cloned.1.call-start = ((), (), s32[]{:S(2)}) async-start(), calls=%async_computation.4 | async-start | bytes 1769472 | tf_op jit(solution)/shard_map/reduce_scatter | solution.py:57
  23.2 3.4 %copy-start.5 = (s32[16,2]{0,1:T(2,128)S(1)}, s32[16,2]{0,1:T(2,128)}, u32[]{:S(2)}) copy-start(s32[16,2]{0,1:T(2,128)} %param.35) | copy-start | bytes 388
  26.5 101.4 %all-reduce.2.cloned.1.call-start = ((), (), s32[]{:S(2)}) async-start(), calls=%async_computation.5 | async-start | bytes 262144 | tf_op jit(solution)/shard_map/psum | solution.py:116
  27.2 10.6 %copy-start.3 = (bf16[4096,64]{0,1:T(8,128)(2,1)S(1)}, bf16[4096,64]{0,1:T(8,128)(2,1)}, u32[]{:S(2)}) copy-start(bf16[4096,64]{0,1:T(8,128)(2,1)} %param.26) | copy-start | bytes 1572868
  69.6 14.1 %copy-start.6 = (f32[256]{0:T(256)S(1)}, f32[256]{0:T(256)}, u32[]{:S(2)}) copy-start(f32[256]{0:T(256)} %param.29) | copy-start | bytes 3076
  83.8 44.1 %copy-start.2 = (bf16[16,4096]{1,0:T(8,128)(2,1)S(1)}, bf16[16,4096]{1,0:T(8,128)(2,1)}, u32[]{:S(2)}) copy-start(bf16[16,4096]{1,0:T(8,128)(2,1)} %param.19) | copy-start | bytes 393220
  83.8 45.1 %copy-start.4 = (f32[4096]{0:T(1024)S(1)}, f32[4096]{0:T(1024)}, u32[]{:S(2)}) copy-start(f32[4096]{0:T(1024)} %param.31) | copy-start | bytes 49156
  83.8 50.9 %copy-start.7 = (f32[16,2]{0,1:T(2,128)S(1)}, f32[16,2]{0,1:T(2,128)}, u32[]{:S(2)}) copy-start(f32[16,2]{0,1:T(2,128)} %param.36) | copy-start | bytes 388
  83.8 50.9 %copy-start.8 = (f32[16]{0:T(128)S(1)}, f32[16]{0:T(128)}, u32[]{:S(2)}) copy-start(f32[16]{0:T(128)} %param.37) | copy-start | bytes 196
  130.1 35.7 %all-to-all-start.1 = ((bf16[8,8,4096]{2,1,0:T(8,128)(2,1)}), bf16[8,8,4096]{2,1,0:T(8,128)(2,1)}, u32[]{:S(2)}, u32[]{:S(2)}) async-start(bf16[8,8,4096]{2,1,0:T(8,128)(2,1)} %fusion.2), calls=%async_computation.2 | async-start | bytes 1048576 | tf_op jit(solution)/shard_map/all_to_all | solution.py:142
  139.4 11.1 %copy-start.1 = (f32[16,128,4]{2,1,0:T(8,128)S(1)}, f32[16,128,4]{2,1,0:T(8,128)}, u32[]{:S(2)}) copy-start(f32[16,128,4]{2,1,0:T(8,128)} %copy.41) | copy-start | bytes 98308
  180.9 18.7 %all-to-all-start.2 = ((bf16[8,8,1024]{2,1,0:T(8,128)(2,1)}), bf16[8,8,1024]{2,1,0:T(8,128)(2,1)S(1)}, u32[]{:S(2)}, u32[]{:S(2)}) async-start(bf16[8,8,1024]{2,1,0:T(8,128)(2,1)} %fusion.17), calls=%async_computation.3 | async-start | bytes 262144 | tf_op jit(solution)/shard_map/all_to_all | solution.py:161
Sparse Core Ops, SparseCore 0:
  26.6 33.2 reduce-scatter.1
  89.3 38.5 all-reduce.1
where the time goes:
time: 209 us; the launch traced here: 207 us
  waiting for transfers between devices  64.4 us (31%)
  local copies, waits for them, and re-layouts  45.8 us (22%)
  other arithmetic  25.8 us (12%)
  matrix products  21.6 us (10%)
  blocking collectives  19.2 us (9%)
  starting transfers between devices  16.1 us (8%)
  between operations  14.3 us (7%)
    psum x1, waiting for transfers between devices, on_device(): lax.psum(partial_out.astype(jnp.bfloat16), 'tp').astype(jnp.float32)  38.6 us
    mul x5, local copies, waits for them, and re-layouts, on_device(): updated = factor * state_four + key_part * value_part  30.7 us
    reduce_scatter x1, waiting for transfers between devices, on_device(): lax.psum_scatter(jnp.dot(spread, joined, preferred_element_type=jnp.float...  20.4 us
    add x2, other arithmetic, on_device(): updated = factor * state_four + key_part * value_part  20 us
    reshape x1, local copies, waits for them, and re-layouts, on_device(): previous_state.reshape(seq_count, KEY_CHANNELS, head_count, head_width)  10.6 us
    psum x1, blocking collectives, on_device(): totals = lax.psum(norm_table, 'tp')  10.2 us
    all_gather x1, blocking collectives, on_device(): lax.all_gather(hidden, 'tp', axis=3, tiled=True)  8.93 us
    all_to_all x1, starting transfers between devices, on_device(): lax.all_to_all(normed, 'ep', split_axis=1, concat_axis=0, tiled=True)  6.35 us
  transfers between devices with their start and end apart: 5, of which 3 were waited for; matrix products, arithmetic and copies ran while one was open for 28% of the time, Pallas kernels for 0%

commit v1 on v0

--- a/solution.py
+++ b/solution.py
@@ -1,11 +1,15 @@
 import jax
 import jax.numpy as jnp
 from jax import lax
+from jax.experimental import pallas as pl
+from jax.experimental.pallas import tpu as pltpu
 from jax.sharding import PartitionSpec as P
 
 HEAD_TOTAL = 16
 KEY_CHANNELS = 128
 DV = 256
+GROUPS = 4
+CORES = 2
 
 
 epsilon = 1e-06
@@ -18,7 +22,7 @@
     return (scaled * gain_vec).astype(jnp.bfloat16)
 
 
-def on_device(
+def on_device_general(
     stream,
     previous_state,
     mixer_norm_gain,
@@ -169,6 +173,353 @@
     return (new_stream, updated.reshape(seq_count, KEY_CHANNELS, value_local))
 
 
+def f32(x):
+    return x.astype(jnp.float32)
+
+
+def bf16(x):
+    return x.astype(jnp.bfloat16)
+
+
+def exchange(x, axis, offset):
+    size = lax.axis_size(axis)
+    return lax.ppermute(x, axis, [(k, k ^ offset) for k in range(size)])
+
+
+def project_kernel(tp_ref, *refs):
+    piece_count = len(refs) - 7
+    pieces = refs[:piece_count]
+    gain, wq, wk, wv, wg, keep, send = refs[piece_count:]
+    rows = pieces[0].shape[0] // CORES
+    width = wq.shape[1]
+    span = wv.shape[1]
+    scaled = [bf16(f32(p[...]) * gain[...]) for p in pieces]
+    x = jnp.concatenate(
+        [p[:rows] for p in scaled] + [p[rows:] for p in scaled], axis=0
+    )
+    half = x.shape[0] // CORES
+    start = 0
+    for w in (wq, wk, wv, wg):
+        y = jnp.dot(x, w[...], preferred_element_type=jnp.float32)
+        keep[:, start : start + w.shape[1]] = bf16(y[:half])
+        send[:, start : start + w.shape[1]] = bf16(y[half:])
+        start += w.shape[1]
+
+
+def project(tp_index, pieces, gain, wq, wk, wv, wg):
+    heads = wv.shape[1] // DV
+    features = wq.shape[0]
+    rows = pieces[0].shape[0] * len(pieces) // CORES
+    head_span = 2 * KEY_CHANNELS + 2 * DV
+    own = lambda j, t: (0, t[0] * heads + j)
+    local = lambda j, t: (0, j)
+    whole = lambda j, t: (0, 0)
+    out = jax.ShapeDtypeStruct((rows, heads * head_span), jnp.bfloat16)
+    return pl.pallas_call(
+        project_kernel,
+        grid_spec=pltpu.PrefetchScalarGridSpec(
+            num_scalar_prefetch=1,
+            grid=(heads,),
+            in_specs=[pl.BlockSpec(p.shape, whole) for p in pieces]
+            + [
+                pl.BlockSpec((1, features), whole),
+                pl.BlockSpec((features, KEY_CHANNELS), own),
+                pl.BlockSpec((features, KEY_CHANNELS), own),
+                pl.BlockSpec((features, DV), local),
+                pl.BlockSpec((features, DV), local),
+            ],
+            out_specs=[pl.BlockSpec((rows, head_span), local)] * 2,
+        ),
+        out_shape=[out, out],
+        name="project",
+    )(tp_index.reshape(1), *pieces, gain.reshape(1, features), wq, wk, wv, wg)
+
+
+def as_columns(row, heads):
+    parts = [row[:, h * KEY_CHANNELS : (h + 1) * KEY_CHANNELS] for h in range(heads)]
+    pad = jnp.zeros((-heads % 8, KEY_CHANNELS), jnp.float32)
+    return jnp.concatenate(parts + [pad], axis=0).T
+
+
+def readout_kernel(*refs):
+    piece_count = len(refs) - 12
+    pieces = refs[:piece_count]
+    (row_scale, decay, head_gain, state, gated, key_out, value_out, qd, qk, gate, read, _) = refs[
+        piece_count:
+    ]
+    step = pl.program_id(0)
+    heads = value_out.shape[1] // DV
+    head_span = 2 * KEY_CHANNELS + 2 * DV
+    per_step = state.shape[0]
+
+    @pl.when(step == 0)
+    def _():
+        for h in range(heads):
+            base = h * head_span
+            total = f32(pieces[0][:, base : base + head_span])
+            for p in pieces[1:]:
+                total = total + f32(p[:, base : base + head_span])
+            total = total * row_scale[...]
+            q = f32(bf16(total[:, :KEY_CHANNELS] * KEY_CHANNELS ** (-0.5)))
+            k = f32(bf16(total[:, KEY_CHANNELS : 2 * KEY_CHANNELS]))
+            v = f32(bf16(total[:, 2 * KEY_CHANNELS : 2 * KEY_CHANNELS + DV]))
+            g = f32(bf16(total[:, 2 * KEY_CHANNELS + DV :]))
+            ks = slice(h * KEY_CHANNELS, (h + 1) * KEY_CHANNELS)
+            vs = slice(h * DV, (h + 1) * DV)
+            key_out[:, ks] = k
+            value_out[:, vs] = v
+            qd[:, ks] = q * decay[:, ks]
+            qk[:, vs] = jnp.sum(q * k, axis=-1, keepdims=True) * v
+            gate[:, vs] = g / (1.0 + jnp.exp(-g))
+
+    for j in range(per_step):
+        s = step * per_step + j
+        cols = as_columns(qd[pl.ds(s, 1), :], heads)
+        for h in range(heads):
+            vs = slice(h * DV, (h + 1) * DV)
+            prod = cols[:, h : h + 1] * state[j, :, vs]
+            read[pl.ds(s, 1), vs] = jnp.sum(prod, axis=0, keepdims=True)
+
+    @pl.when(step == pl.num_programs(0) - 1)
+    def _():
+        for h in range(heads):
+            vs = slice(h * DV, (h + 1) * DV)
+            r = read[:, vs] + qk[:, vs]
+            inv = lax.rsqrt(jnp.mean(r * r, axis=-1, keepdims=True) + epsilon)
+            gated[:, vs] = bf16(r * inv * head_gain[...] * gate[:, vs])
+
+
+def readout_call(pieces, row_scale, decay, head_gain, state):
+    seqs, channels, values = state.shape
+    keys = decay.shape[1]
+    per_step = 2
+    whole = lambda i: (0, 0)
+    full = lambda a: pl.BlockSpec(a.shape, whole)
+    return pl.pallas_call(
+        readout_kernel,
+        grid=(seqs // per_step,),
+        in_specs=[full(p) for p in pieces]
+        + [full(row_scale), full(decay), full(head_gain)]
+        + [pl.BlockSpec((per_step, channels, values), lambda i: (i, 0, 0))],
+        out_specs=[
+            pl.BlockSpec((seqs, values), whole),
+            pl.BlockSpec((seqs, keys), whole),
+            pl.BlockSpec((seqs, values), whole),
+        ],
+        out_shape=[
+            jax.ShapeDtypeStruct((seqs, values), jnp.bfloat16),
+            jax.ShapeDtypeStruct((seqs, keys), jnp.float32),
+            jax.ShapeDtypeStruct((seqs, values), jnp.float32),
+        ],
+        scratch_shapes=[
+            pltpu.VMEM((seqs, keys), jnp.float32),
+            pltpu.VMEM((seqs, values), jnp.float32),
+            pltpu.VMEM((seqs, values), jnp.float32),
+            pltpu.VMEM((seqs, values), jnp.float32),
+            pltpu.VMEM((8, 128), jnp.float32),
+        ],
+        name="readout",
+    )(*pieces, row_scale, decay, head_gain, state)
+
+
+def state_kernel(decay, keys, values, state, out):
+    step = pl.program_id(0)
+    per_step = state.shape[0]
+    heads = values.shape[1] // DV
+    for j in range(per_step):
+        s = step * per_step + j
+        decay_cols = as_columns(decay[pl.ds(s, 1), :], heads)
+        key_cols = as_columns(keys[pl.ds(s, 1), :], heads)
+        value_row = values[pl.ds(s, 1), :]
+        for h in range(heads):
+            vs = slice(h * DV, (h + 1) * DV)
+            out[j, :, vs] = (
+                decay_cols[:, h : h + 1] * state[j, :, vs]
+                + key_cols[:, h : h + 1] * value_row[:, vs]
+            )
+
+
+def state_call(decay, keys, values, state):
+    seqs, channels, width = state.shape
+    per_step = 2
+    block = pl.BlockSpec((per_step, channels, width), lambda i: (i, 0, 0))
+    full = lambda a: pl.BlockSpec(a.shape, lambda i: (0, 0))
+    return pl.pallas_call(
+        state_kernel,
+        grid=(seqs // per_step,),
+        in_specs=[full(decay), full(keys), full(values), block],
+        out_specs=block,
+        out_shape=jax.ShapeDtypeStruct(state.shape, jnp.float32),
+        cost_estimate=pl.CostEstimate(
+            flops=40 * state.size, bytes_accessed=8 * state.size, transcendentals=0
+        ),
+        name="state_update",
+    )(decay, keys, values, state)
+
+
+def on_device_paired(
+    stream,
+    previous_state,
+    mixer_norm_gain,
+    query_matrix,
+    key_matrix,
+    value_matrix,
+    output_gate_weight,
+    decay_lower_factor,
+    decay_upper_factor,
+    forgetting_boost,
+    head_norm_gain,
+    output_matrix,
+    mixture_norm_gain,
+    expert_gate_weight,
+    expert_up_weight,
+    expert_down_weight,
+    expert_index_table,
+    expert_scores_within,
+    group_probability,
+):
+    seq_count, model_width = stream.shape
+    value_local = previous_state.shape[2]
+    head_count = value_local // DV
+    ep_count = lax.axis_size("ep")
+    tp_count = lax.axis_size("tp")
+    chips = ep_count // CORES
+    tp_index = lax.axis_index("tp")
+    ep_index = lax.axis_index("ep")
+    chip, core = ep_index // CORES, ep_index % CORES
+    key_column_span = head_count * KEY_CHANNELS
+    first_key = tp_index * key_column_span
+    features = query_matrix.shape[0]
+
+    partner_stream = exchange(stream, "ep", 1)
+    pieces = []
+    for d in range(chips):
+        start = ((chip ^ d) * CORES + core) * features
+        both = [lax.dynamic_slice_in_dim(a, start, features, 1) for a in (stream, partner_stream)]
+        block = jnp.concatenate(both, axis=0)
+        pieces.append(exchange(block, "ep", CORES * d) if d else block)
+    own_gain = lax.dynamic_slice_in_dim(mixer_norm_gain, ep_index * features, features, 0)
+    keep, send = project(
+        tp_index, pieces, own_gain, query_matrix, key_matrix, value_matrix, output_gate_weight
+    )
+    on_chip = bf16(f32(keep) + f32(exchange(send, "ep", 1)))
+    sums = []
+    for d in range(chips):
+        block = on_chip[d * seq_count : (d + 1) * seq_count]
+        sums.append(exchange(block, "ep", CORES * d) if d else block)
+
+    floats = f32(stream)
+    row_scale = lax.rsqrt(jnp.mean(floats * floats, axis=-1, keepdims=True) + epsilon)
+    normed = bf16(floats * row_scale * mixer_norm_gain)
+    low_rank = bf16(jnp.dot(normed, decay_lower_factor, preferred_element_type=jnp.float32))
+    local_upper = lax.dynamic_slice_in_dim(decay_upper_factor, first_key, key_column_span, 1)
+    logit = jnp.dot(low_rank, local_upper, preferred_element_type=jnp.float32)
+    boost = lax.dynamic_slice_in_dim(forgetting_boost, first_key, key_column_span, 1)
+    decay = jnp.exp(jax.nn.log_sigmoid(logit) / forgetting_softness - boost)
+
+    gated_rows, key_rows, value_rows = readout_call(
+        sums, row_scale, decay, head_norm_gain.reshape(1, DV), previous_state
+    )
+    partial_out = bf16(jnp.dot(gated_rows, output_matrix, preferred_element_type=jnp.float32))
+    mixed = floats + f32(partial_out)
+    for d in range(1, tp_count):
+        mixed = mixed + f32(exchange(partial_out, "tp", d))
+    new_state = state_call(decay, key_rows, value_rows, previous_state)
+    mixed = bf16(mixed)
+    normed_two = rms_scaled(mixed, mixture_norm_gain)
+
+    route_count = expert_index_table.shape[1]
+    capacity = 2 * seq_count * route_count // (ep_count * expert_gate_weight.shape[0])
+    slot_count = chips * capacity
+    relative = (expert_index_table[:, 0] // CORES) ^ chip
+    in_group = (relative[:, None] == jnp.arange(chips, dtype=jnp.int32)[None, :]).astype(jnp.int32)
+    earlier = (
+        jnp.arange(seq_count, dtype=jnp.int32)[:, None]
+        > jnp.arange(seq_count, dtype=jnp.int32)[None, :]
+    )
+    same = relative[:, None] == relative[None, :]
+    rank = jnp.sum((earlier & same).astype(jnp.int32), axis=1)
+    place = relative * capacity + rank
+    placing = place[:, None] == jnp.arange(slot_count, dtype=jnp.int32)[None, :]
+    logit_exp = jnp.exp(expert_scores_within)
+    weights = logit_exp / jnp.sum(logit_exp, axis=-1, keepdims=True) * group_probability[:, None]
+    at_core = expert_index_table % CORES
+    combine = jnp.stack(
+        [
+            jnp.where(
+                placing,
+                jnp.sum(jnp.where(at_core == which, weights, 0.0), axis=1, keepdims=True),
+                0.0,
+            ).reshape(seq_count, chips, capacity)
+            for which in (core, 1 - core)
+        ],
+        axis=2,
+    ).reshape(seq_count, CORES * slot_count)
+    outgoing = bf16(
+        jnp.einsum(
+            "sc,sd->cd", bf16(placing), normed_two, preferred_element_type=jnp.float32
+        )
+    )
+    arrived = []
+    for d in range(chips):
+        block = outgoing[d * capacity : (d + 1) * capacity]
+        arrived.append(exchange(block, "ep", CORES * d) if d else block)
+    arrived = jnp.concatenate(arrived, axis=0)
+    rows = jnp.concatenate([arrived, exchange(arrived, "ep", 1)], axis=0)
+
+    contract_last = (((1,), (1,)), ((), ()))
+    gate_pre = lax.dot_general(
+        rows, expert_gate_weight[0], contract_last, preferred_element_type=jnp.float32
+    )
+    up_pre = lax.dot_general(
+        rows, expert_up_weight[0], contract_last, preferred_element_type=jnp.float32
+    )
+    hidden = bf16(jax.nn.silu(gate_pre) * up_pre)
+    parts = jnp.stack([hidden] + [exchange(hidden, "tp", d) for d in range(1, tp_count)])
+    hidden_all = jnp.concatenate(
+        [
+            lax.dynamic_index_in_dim(parts, tp_index ^ j, 0, keepdims=False)
+            for j in range(tp_count)
+        ],
+        axis=1,
+    )
+    outputs = bf16(
+        jnp.dot(hidden_all, expert_down_weight[0], preferred_element_type=jnp.float32)
+    )
+    width_local = outputs.shape[1]
+    same_core = outputs[:slot_count].reshape(chips, capacity, width_local)
+    other_core = exchange(outputs[slot_count:], "ep", 1).reshape(chips, capacity, width_local)
+    back = []
+    for d in range(chips):
+        block = jnp.concatenate([same_core[d], other_core[d]], axis=0)
+        back.append(exchange(block, "ep", CORES * d) if d else block)
+    mixture = jnp.dot(
+        combine, f32(jnp.concatenate(back, axis=0)), precision=lax.Precision.HIGHEST
+    )
+    own_mixed = lax.dynamic_slice_in_dim(mixed, tp_index * width_local, width_local, 1)
+    new_stream = bf16(f32(own_mixed) + mixture)
+    return (new_stream, new_state)
+
+
+def power_of_two(n):
+    return n & (n - 1) == 0
+
+
+def on_device(*args):
+    values, local_experts = args[1].shape[2], args[13].shape[0]
+    ep_count, tp_count = lax.axis_size("ep"), lax.axis_size("tp")
+    per_group = ep_count * local_experts // GROUPS
+    paired = (
+        values % DV == 0
+        and local_experts == 1
+        and per_group == CORES
+        and args[16].shape[1] == CORES
+        and power_of_two(ep_count)
+        and power_of_two(tp_count)
+    )
+    return (on_device_paired if paired else on_device_general)(*args)
+
+
 def solution(mesh):
     placed = (
         P("ep", None),

time: 209 us -> 97.6 us (0.47)
  local copies, waits for them, and re-layouts: 45.8 us -> 4.91 us
  waiting for transfers between devices: 64.4 us -> 27.2 us
  Pallas kernels: 0 us -> 22.8 us
  other arithmetic: 25.8 us -> 4.81 us
  blocking collectives: 19.2 us -> 0 us
  between operations: 14.3 us -> 0.96 us
  matrix products: 21.6 us -> 9.77 us
  starting transfers between devices: 16.1 us -> 26.4 us
    psum x1 -> x0, waiting for transfers between devices: 38.6 us -> none  [on_device(): lax.psum(partial_out.astype(jnp.bfloat16), 'tp').astype(jnp.float32)]
    mul x6 -> x0, local copies, waits for them, and re-layouts: 30.8 us -> none  [the longest x5 30.7 us: on_device(): updated = factor * state_four + key_part * value_part]
    ppermute x0 -> x22, waiting for transfers between devices: none -> 27.2 us  [exchange(): return lax.ppermute(x, axis, [(k, k ^ offset) for k in range(size)])]
    ppermute x0 -> x22, starting transfers between devices: none -> 26.4 us  [exchange(): return lax.ppermute(x, axis, [(k, k ^ offset) for k in range(size)])]
    pallas_call x0 -> x3, Pallas kernels: none -> 22.8 us  [the longest x1 10.7 us: state_call(): pl.pallas_call(state_kernel, grid=(seqs // per_step,), in_specs=[full(dec...]
    reduce_scatter x1 -> x0, waiting for transfers between devices: 20.4 us -> none  [on_device(): lax.psum_scatter(jnp.dot(spread, joined, preferred_element_type=jnp.float...]
    add x3 -> x0, other arithmetic: 20 us -> none  [the longest x2 20 us: on_device(): updated = factor * state_four + key_part * value_part]
    all_to_all x3 -> x0, starting transfers between devices: 16.1 us -> none  [the longest x1 6.35 us: on_device(): lax.all_to_all(normed, 'ep', split_axis=1, concat_axis=0, tiled=True)]
  transfers between devices with their start and end apart: 5 -> 22, of which waited for: 3 -> 13; matrix products, arithmetic and copies ran while one was open for 28% -> 9% of each run, Pallas kernels for 0% -> 11%
where the time goes in v1:
time: 97.6 us; the launch traced here: 96.9 us
  waiting for transfers between devices  27.2 us (28%)
  starting transfers between devices  26.4 us (27%)
  Pallas kernels  22.8 us (23%)
  matrix products  9.77 us (10%)
  local copies, waits for them, and re-layouts  4.91 us (5%)
  other arithmetic  4.81 us (5%)
    ppermute x22, waiting for transfers between devices, exchange(): return lax.ppermute(x, axis, [(k, k ^ offset) for k in range(size)])  27.2 us
    ppermute x22, starting transfers between devices, exchange(): return lax.ppermute(x, axis, [(k, k ^ offset) for k in range(size)])  26.4 us
    pallas_call x1, Pallas kernels, state_call(): pl.pallas_call(state_kernel, grid=(seqs // per_step,), in_specs=[full(dec...  10.7 us
    pallas_call x1, Pallas kernels, readout_call(): pl.pallas_call(readout_kernel, grid=(seqs // per_step,), in_specs=[full(p...  7.74 us
    dot_general x1, matrix products, on_device_paired(): jnp.dot(gated_rows, output_matrix, preferred_element_type=jnp.float32)  4.62 us
    pallas_call x1, Pallas kernels, project(): pl.pallas_call(project_kernel, grid_spec=pltpu.PrefetchScalarGridSpec(num...  4.36 us
    dot_general x1, matrix products, on_device_paired(): logit = jnp.dot(low_rank, local_upper, preferred_element_type=jnp.float32)  1.95 us
  transfers between devices with their start and end apart: 22, of which 13 were waited for; matrix products, arithmetic and copies ran while one was open for 9% of the time, Pallas kernels for 11%

profile of v1, /device:TPU:0, one launch (start us, length us, event | category | flops | bytes accessed | tf_op | source)
XLA Modules:
  0.0 96.9 jit_solution(2536962764593177012)
XLA Ops:
  2.6 1.0 %fusion.12 = f32[16]{0:T(128)S(1)} fusion(bf16[16,4096]{1,0:T(8,128)(2,1)} %param.19), kind=kLoop, calls=%fused_computation.20 | loop fusion | flops 196592 | bytes 131136 | tf_op jit(solution)/shard_map/reduce_sum | solution.py:412
  4.6 1.3 %dynamic_slice.57 = f32[512]{0:T(512)} dynamic-slice(f32[4096]{0:T(1024)} %param.21, s32[]{:T(128)S(6)} %select_n.108), dynamic_slice_sizes={512} | dynamic-slice | bytes 4100 | tf_op jit(solution)/shard_map/dynamic_slice | solution.py:401
  5.9 0.8 constant_dynamic-slice_fusion.1
  6.8 2.7 %collective-permute-start.1 = (bf16[32,512]{1,0:T(8,128)(2,1)S(1)}, bf16[32,512]{1,0:T(8,128)(2,1)S(1)}, u32[]{:S(2)}, u32[]{:S(2)}) collective-permute-start(bf16[32,512]{1,0:T(8,128)(2,1)S(1)} %pad_maximum_fusion.3), channel_id=1, source_target_pairs={{0,8},{4,12},{8,0},{12,4},{16,24},{20,28},{24,16},{28,20},{1,9},{5... | collective-permute-start | bytes 98312 | tf_op jit(solution)/shard_map/ppermute | solution.py:186
  9.5 2.6 %collective-permute-start.2 = (bf16[32,512]{1,0:T(8,128)(2,1)S(1)}, bf16[32,512]{1,0:T(8,128)(2,1)S(1)}, u32[]{:S(2)}, u32[]{:S(2)}) collective-permute-start(bf16[32,512]{1,0:T(8,128)(2,1)S(1)} %pad_maximum_fusion.4), channel_id=1, source_target_pairs={{0,16},{4,20},{8,24},{12,28},{16,0},{20,4},{24,8},{28,12},{1,17},{... | collective-permute-start | bytes 98312 | tf_op jit(solution)/shard_map/ppermute | solution.py:186
  12.7 2.2 %collective-permute-done.2.refs_2_ = bf16[32,512]{1,0:T(8,128)(2,1)S(1)} collective-permute-done((bf16[32,512]{1,0:T(8,128)(2,1)S(1)}, bf16[32,512]{1,0:T(8,128)(2,1)S(1)}, u32[]{:S(2)}, u32[]{:S(2)}) %collective-permute-start.2) | collective-permute-done | bytes 32800 | tf_op jit(solution)/shard_map/ppermute | solution.py:186
  14.9 2.9 %collective-permute-done.3.refs_3_ = bf16[32,512]{1,0:T(8,128)(2,1)S(1)} collective-permute-done((bf16[32,512]{1,0:T(8,128)(2,1)S(1)}, bf16[32,512]{1,0:T(8,128)(2,1)S(1)}, u32[]{:S(2)}, u32[]{:S(2)}) %collective-permute-start.3) | collective-permute-done | bytes 32800 | tf_op jit(solution)/shard_map/ppermute | solution.py:186
  18.4 4.4 %project.1 = (bf16[64,3072]{1,0:T(8,128)(2,1)}, bf16[64,3072]{1,0:T(8,128)(2,1)}) custom-call(s32[1]{0:T(128)} %bitcast.tp_ref, bf16[32,512]{1,0:T(8,128)(2,1)} %pad_maximum_fusion.2.refs_0_, bf16[32,512]{1,0:T(8,128)(2,1)} %copy-done.8, bf16[32,512]{1,0:T(8,128)(2,1)} %copy-done.9, bf16[32,512]{1,0:T(8,128)(2,1)} %copy-done.10, f32[1,512]{1,0:T(1,128)} %bitcast.61, ...), custom_call_target="tpu_custom_call" | custom-call | tf_op jit(solution)/shard_map/project/pallas_call | solution.py:218
  22.9 2.0 %fusion.39.refs_5_.decay = f32[16,512]{1,0:T(8,128)} fusion(f32[16,2048]{1,0:T(8,128)} %param.28, s32[]{:T(128)S(6)} %select_n.109, bf16[64,2048]{1,0:T(8,128)(2,1)} %param.27, bf16[4096,64]{0,1:T(8,128)(2,1)S(1)} %copy-done.4, bf16[16,4096]{1,0:T(8,128)(2,1)S(1)} %copy-done.3, f32[4096]{0:T(1024)S(1)} %copy-done.11, f32[16]{0:T(128)S(1)} %get-tuple-element.47), kind=kOutput, calls=%fused_computation.47 | convolution fusion | flops 9782272 | bytes 803904 | tf_op jit(solution)/shard_map/dot_general | solution.py:416
  24.9 1.1 %add_convert_fusion = bf16[64,3072]{1,0:T(8,128)(2,1)S(1)} fusion(bf16[64,3072]{1,0:T(8,128)(2,1)S(1)} %collective-permute-done.4, bf16[64,3072]{1,0:T(8,128)(2,1)} %get-tuple-element.7), kind=kLoop, calls=%fused_computation.11 | loop fusion | flops 786432 | bytes 1179648 | tf_op jit(solution)/shard_map/convert_element_type | solution.py:181
  27.1 4.0 %collective-permute-start.5 = (bf16[16,3072]{1,0:T(8,128)(2,1)S(1)}, bf16[16,3072]{1,0:T(8,128)(2,1)S(1)}, u32[]{:S(2)}, u32[]{:S(2)}) collective-permute-start(bf16[16,3072]{1,0:T(8,128)(2,1)S(1)} %get-tuple-element.18), channel_id=1, source_target_pairs={{0,8},{4,12},{8,0},{12,4},{16,24},{20,28},{24,16},{28,20},{1,9},{5... | collective-permute-start | bytes 294920 | tf_op jit(solution)/shard_map/ppermute | solution.py:186
  31.1 3.2 %collective-permute-done.7.refs_3_ = bf16[16,3072]{1,0:T(8,128)(2,1)S(1)} collective-permute-done((bf16[16,3072]{1,0:T(8,128)(2,1)S(1)}, bf16[16,3072]{1,0:T(8,128)(2,1)S(1)}, u32[]{:S(2)}, u32[]{:S(2)}) %collective-permute-start.7) | collective-permute-done | bytes 98336 | tf_op jit(solution)/shard_map/ppermute | solution.py:186
  34.2 2.9 %collective-permute-done.6.refs_2_ = bf16[16,3072]{1,0:T(8,128)(2,1)S(1)} collective-permute-done((bf16[16,3072]{1,0:T(8,128)(2,1)S(1)}, bf16[16,3072]{1,0:T(8,128)(2,1)S(1)}, u32[]{:S(2)}, u32[]{:S(2)}) %collective-permute-start.6) | collective-permute-done | bytes 98336 | tf_op jit(solution)/shard_map/ppermute | solution.py:186
  37.7 7.7 %readout.1 = (bf16[16,1024]{1,0:T(8,128)(2,1)}, f32[16,512]{1,0:T(8,128)}, f32[16,1024]{1,0:T(8,128)}) custom-call(bf16[16,3072]{1,0:T(8,128)(2,1)} %get-tuple-element.19.refs_0_, bf16[16,3072]{1,0:T(8,128)(2,1)} %copy-done.7, bf16[16,3072]{1,0:T(8,128)(2,1)} %copy-done.6, bf16[16,3072]{1,0:T(8,128)(2,1)} %copy-done.5, f32[16,1]{1,0:T(8,128)} %copy.23.refs_4_, ...), custom_call_target="tpu_custom_call" | custom-call | tf_op jit(solution)/shard_map/readout/pallas_call | solution.py:298
  45.5 4.6 %convolution_convert_fusion.1 = bf16[16,4096]{1,0:T(8,128)(2,1)S(1)} fusion(bf16[16,1024]{1,0:T(8,128)(2,1)} %get-tuple-element.9, bf16[1024,4096]{1,0:T(8,128)(2,1)} %param.30), kind=kOutput, calls=%fused_computation.1 | convolution fusion | flops 134283264 | bytes 8552448 | tf_op jit(solution)/shard_map/dot_general | solution.py:423
  50.1 2.5 %collective-permute-start.10 = (bf16[16,4096]{1,0:T(8,128)(2,1)S(1)}, bf16[16,4096]{1,0:T(8,128)(2,1)S(1)}, u32[]{:S(2)}, u32[]{:S(2)}) collective-permute-start(bf16[16,4096]{1,0:T(8,128)(2,1)S(1)} %convolution_convert_fusion.1), channel_id=1, source_target_pairs={{0,3},{1,2},{2,1},{3,0},{4,7},{5,6},{6,5},{7,4},{8,11},{9,10},{10,... | collective-permute-start | bytes 393224 | tf_op jit(solution)/shard_map/ppermute | solution.py:186
  53.7 2.9 %collective-permute-done.10 = bf16[16,4096]{1,0:T(8,128)(2,1)S(1)} collective-permute-done((bf16[16,4096]{1,0:T(8,128)(2,1)S(1)}, bf16[16,4096]{1,0:T(8,128)(2,1)S(1)}, u32[]{:S(2)}, u32[]{:S(2)}) %collective-permute-start.10) | collective-permute-done | bytes 131104 | tf_op jit(solution)/shard_map/ppermute | solution.py:186
  56.6 2.0 %collective-permute-done.9 = bf16[16,4096]{1,0:T(8,128)(2,1)S(1)} collective-permute-done((bf16[16,4096]{1,0:T(8,128)(2,1)S(1)}, bf16[16,4096]{1,0:T(8,128)(2,1)S(1)}, u32[]{:S(2)}, u32[]{:S(2)}) %collective-permute-start.9) | collective-permute-done | bytes 131104 | tf_op jit(solution)/shard_map/ppermute | solution.py:186
  59.3 2.1 %collective-permute-start.13 = (bf16[8,4096]{1,0:T(8,128)(2,1)S(1)}, bf16[8,4096]{1,0:T(8,128)(2,1)S(1)}, u32[]{:S(2)}, u32[]{:S(2)}) collective-permute-start(bf16[8,4096]{1,0:T(8,128)(2,1)S(1)} %get-tuple-element.22), channel_id=1, source_target_pairs={{0,24},{4,28},{8,16},{12,20},{16,8},{20,12},{24,0},{28,4},{1,25},{... | collective-permute-start | bytes 196616 | tf_op jit(solution)/shard_map/ppermute | solution.py:186
  61.4 2.3 %collective-permute-start.11 = (bf16[8,4096]{1,0:T(8,128)(2,1)S(1)}, bf16[8,4096]{1,0:T(8,128)(2,1)S(1)}, u32[]{:S(2)}, u32[]{:S(2)}) collective-permute-start(bf16[8,4096]{1,0:T(8,128)(2,1)S(1)} %get-tuple-element.24), channel_id=1, source_target_pairs={{0,8},{4,12},{8,0},{12,4},{16,24},{20,28},{24,16},{28,20},{1,9},{5... | collective-permute-start | bytes 196616 | tf_op jit(solution)/shard_map/ppermute | solution.py:186
  63.8 1.7 %collective-permute-done.13 = bf16[8,4096]{1,0:T(8,128)(2,1)S(1)} collective-permute-done((bf16[8,4096]{1,0:T(8,128)(2,1)S(1)}, bf16[8,4096]{1,0:T(8,128)(2,1)S(1)}, u32[]{:S(2)}, u32[]{:S(2)}) %collective-permute-start.13) | collective-permute-done | bytes 65568 | tf_op jit(solution)/shard_map/ppermute | solution.py:186
  65.5 2.0 %collective-permute-done.12 = bf16[8,4096]{1,0:T(8,128)(2,1)S(1)} collective-permute-done((bf16[8,4096]{1,0:T(8,128)(2,1)S(1)}, bf16[8,4096]{1,0:T(8,128)(2,1)S(1)}, u32[]{:S(2)}, u32[]{:S(2)}) %collective-permute-start.12) | collective-permute-done | bytes 65568 | tf_op jit(solution)/shard_map/ppermute | solution.py:186
  67.6 1.5 %collective-permute-done.14 = bf16[32,4096]{1,0:T(8,128)(2,1)S(1)} collective-permute-done((bf16[32,4096]{1,0:T(8,128)(2,1)S(1)}, bf16[32,4096]{1,0:T(8,128)(2,1)S(1)}, u32[]{:S(2)}, u32[]{:S(2)}) %collective-permute-start.14) | collective-permute-done | bytes 262176 | tf_op jit(solution)/shard_map/ppermute | solution.py:186
  70.7 1.6 %collective-permute-start.17 = (bf16[64,256]{1,0:T(8,128)(2,1)S(1)}, bf16[64,256]{1,0:T(8,128)(2,1)S(1)}, u32[]{:S(2)}, u32[]{:S(2)}) collective-permute-start(bf16[64,256]{1,0:T(8,128)(2,1)S(1)} %multiply_convert_fusion), channel_id=1, source_target_pairs={{0,3},{1,2},{2,1},{3,0},{4,7},{5,6},{6,5},{7,4},{8,11},{9,10},{10,... | collective-permute-start | bytes 98312 | tf_op jit(solution)/shard_map/ppermute | solution.py:186
  72.3 1.4 %collective-permute-start.16 = (bf16[64,256]{1,0:T(8,128)(2,1)S(1)}, bf16[64,256]{1,0:T(8,128)(2,1)S(1)}, u32[]{:S(2)}, u32[]{:S(2)}) collective-permute-start(bf16[64,256]{1,0:T(8,128)(2,1)S(1)} %multiply_convert_fusion), channel_id=1, source_target_pairs={{0,2},{1,3},{2,0},{3,1},{4,6},{5,7},{6,4},{7,5},{8,10},{9,11},{10,... | collective-permute-start | bytes 98312 | tf_op jit(solution)/shard_map/ppermute | solution.py:186
  74.2 10.7 %state_update.1 = f32[16,128,1024]{2,1,0:T(8,128)} custom-call(f32[16,512]{1,0:T(8,128)} %fusion.39.refs_5_.decay, f32[16,512]{1,0:T(8,128)} %get-tuple-element.10.keys, f32[16,1024]{1,0:T(8,128)} %get-tuple-element.11.values, f32[16,128,1024]{2,1,0:T(8,128)} %state.1), custom_call_target="tpu_custom_call" | custom-call | flops 83886080 | bytes 16777216 | tf_op jit(solution)/shard_map/state_update/pallas_call | solution.py:347
  85.7 1.2 %collective-permute-done.18 = bf16[32,1024]{1,0:T(8,128)(2,1)S(1)} collective-permute-done((bf16[32,1024]{1,0:T(8,128)(2,1)S(1)}, bf16[32,1024]{1,0:T(8,128)(2,1)S(1)}, u32[]{:S(2)}, u32[]{:S(2)}) %collective-permute-start.18) | collective-permute-done | bytes 65568 | tf_op jit(solution)/shard_map/ppermute | solution.py:186
  87.6 2.8 %collective-permute-start.20 = (bf16[16,1024]{1,0:T(8,128)(2,1)S(1)}, bf16[16,1024]{1,0:T(8,128)(2,1)S(1)}, u32[]{:S(2)}, u32[]{:S(2)}) collective-permute-start(bf16[16,1024]{1,0:T(8,128)(2,1)S(1)} %pad_maximum_fusion.8), channel_id=1, source_target_pairs={{0,16},{4,20},{8,24},{12,28},{16,0},{20,4},{24,8},{28,12},{1,17},{... | collective-permute-start | bytes 98312 | tf_op jit(solution)/shard_map/ppermute | solution.py:186
  90.3 1.0 %collective-permute-start.21 = (bf16[16,1024]{1,0:T(8,128)(2,1)S(1)}, bf16[16,1024]{1,0:T(8,128)(2,1)S(1)}, u32[]{:S(2)}, u32[]{:S(2)}) collective-permute-start(bf16[16,1024]{1,0:T(8,128)(2,1)S(1)} %pad_maximum_fusion.9), channel_id=1, source_target_pairs={{0,24},{4,28},{8,16},{12,20},{16,8},{20,12},{24,0},{28,4},{1,25},{... | collective-permute-start | bytes 98312 | tf_op jit(solution)/shard_map/ppermute | solution.py:186
  91.4 1.3 %collective-permute-done.20 = bf16[16,1024]{1,0:T(8,128)(2,1)S(1)} collective-permute-done((bf16[16,1024]{1,0:T(8,128)(2,1)S(1)}, bf16[16,1024]{1,0:T(8,128)(2,1)S(1)}, u32[]{:S(2)}, u32[]{:S(2)}) %collective-permute-start.20) | collective-permute-done | bytes 32800 | tf_op jit(solution)/shard_map/ppermute | solution.py:186
  92.7 3.4 %collective-permute-done.21 = bf16[16,1024]{1,0:T(8,128)(2,1)S(1)} collective-permute-done((bf16[16,1024]{1,0:T(8,128)(2,1)S(1)}, bf16[16,1024]{1,0:T(8,128)(2,1)S(1)}, u32[]{:S(2)}, u32[]{:S(2)}) %collective-permute-start.21) | collective-permute-done | bytes 32800 | tf_op jit(solution)/shard_map/ppermute | solution.py:186
  96.1 0.9 add_convert_fusion.1
  (94 shorter events, 11.3 us)
Async XLA Ops:
  0.6 84.4 %copy-start = (bf16[1,1024,1024]{2,1,0:T(8,128)(2,1)S(1)}, bf16[1,1024,1024]{2,1,0:T(8,128)(2,1)}, u32[]{:S(2)}) copy-start(bf16[1,1024,1024]{2,1,0:T(8,128)(2,1)} %param.34) | copy-start | bytes 6291460
  0.6 6.1 %collective-permute-start = (bf16[16,4096]{1,0:T(8,128)(2,1)}, bf16[16,4096]{1,0:T(8,128)(2,1)S(1)}, u32[]{:S(2)}, u32[]{:S(2)}) collective-permute-start(bf16[16,4096]{1,0:T(8,128)(2,1)} %param.19), channel_id=1, source_target_pairs={{0,4},{4,0},{8,12},{12,8},{16,20},{20,16},{24,28},{28,24},{1,5},{5... | collective-permute-start | bytes 393224 | tf_op jit(solution)/shard_map/ppermute | solution.py:186
  6.8 5.9 %collective-permute-start.1 = (bf16[32,512]{1,0:T(8,128)(2,1)S(1)}, bf16[32,512]{1,0:T(8,128)(2,1)S(1)}, u32[]{:S(2)}, u32[]{:S(2)}) collective-permute-start(bf16[32,512]{1,0:T(8,128)(2,1)S(1)} %pad_maximum_fusion.3), channel_id=1, source_target_pairs={{0,8},{4,12},{8,0},{12,4},{16,24},{20,28},{24,16},{28,20},{1,9},{5... | collective-permute-start | bytes 98312 | tf_op jit(solution)/shard_map/ppermute | solution.py:186
  9.5 5.4 %collective-permute-start.2 = (bf16[32,512]{1,0:T(8,128)(2,1)S(1)}, bf16[32,512]{1,0:T(8,128)(2,1)S(1)}, u32[]{:S(2)}, u32[]{:S(2)}) collective-permute-start(bf16[32,512]{1,0:T(8,128)(2,1)S(1)} %pad_maximum_fusion.4), channel_id=1, source_target_pairs={{0,16},{4,20},{8,24},{12,28},{16,0},{20,4},{24,8},{28,12},{1,17},{... | collective-permute-start | bytes 98312 | tf_op jit(solution)/shard_map/ppermute | solution.py:186
  12.1 5.7 %collective-permute-start.3 = (bf16[32,512]{1,0:T(8,128)(2,1)S(1)}, bf16[32,512]{1,0:T(8,128)(2,1)S(1)}, u32[]{:S(2)}, u32[]{:S(2)}) collective-permute-start(bf16[32,512]{1,0:T(8,128)(2,1)S(1)} %pad_maximum_fusion.5), channel_id=1, source_target_pairs={{0,24},{4,28},{8,16},{12,20},{16,8},{20,12},{24,0},{28,4},{1,25},{... | collective-permute-start | bytes 98312 | tf_op jit(solution)/shard_map/ppermute | solution.py:186
  12.7 5.1 %copy-start.8 = (bf16[32,512]{1,0:T(8,128)(2,1)}, bf16[32,512]{1,0:T(8,128)(2,1)S(1)}, u32[]{:S(2)}) copy-start(bf16[32,512]{1,0:T(8,128)(2,1)S(1)} %collective-permute-done.1.refs_1_) | copy-start | bytes 98308
  18.4 4.5 %copy-start.3 = (bf16[16,4096]{1,0:T(8,128)(2,1)S(1)}, bf16[16,4096]{1,0:T(8,128)(2,1)}, u32[]{:S(2)}) copy-start(bf16[16,4096]{1,0:T(8,128)(2,1)} %param.19) | copy-start | bytes 393220
  18.4 4.5 %copy-start.4 = (bf16[4096,64]{0,1:T(8,128)(2,1)S(1)}, bf16[4096,64]{0,1:T(8,128)(2,1)}, u32[]{:S(2)}) copy-start(bf16[4096,64]{0,1:T(8,128)(2,1)} %param.26) | copy-start | bytes 1572868
  18.4 4.5 %copy-start.11 = (f32[4096]{0:T(1024)S(1)}, f32[4096]{0:T(1024)}, u32[]{:S(2)}) copy-start(f32[4096]{0:T(1024)} %param.21) | copy-start | bytes 49156
  22.8 8.3 %copy-start.14 = (f32[16,2]{0,1:T(2,128)S(1)}, f32[16,2]{0,1:T(2,128)}, u32[]{:S(2)}) copy-start(f32[16,2]{0,1:T(2,128)} %param.36) | copy-start | bytes 388
  22.8 2.1 %collective-permute-start.4 = (bf16[64,3072]{1,0:T(8,128)(2,1)}, bf16[64,3072]{1,0:T(8,128)(2,1)S(1)}, u32[]{:S(2)}, u32[]{:S(2)}) collective-permute-start(bf16[64,3072]{1,0:T(8,128)(2,1)} %get-tuple-element.8), channel_id=1, source_target_pairs={{0,4},{4,0},{8,12},{12,8},{16,20},{20,16},{24,28},{28,24},{1,5},{5... | collective-permute-start | bytes 1179656 | tf_op jit(solution)/shard_map/ppermute | solution.py:186
  26.6 7.6 %collective-permute-start.7 = (bf16[16,3072]{1,0:T(8,128)(2,1)S(1)}, bf16[16,3072]{1,0:T(8,128)(2,1)S(1)}, u32[]{:S(2)}, u32[]{:S(2)}) collective-permute-start(bf16[16,3072]{1,0:T(8,128)(2,1)S(1)} %get-tuple-element.16), channel_id=1, source_target_pairs={{0,24},{4,28},{8,16},{12,20},{16,8},{20,12},{24,0},{28,4},{1,25},{... | collective-permute-start | bytes 294920 | tf_op jit(solution)/shard_map/ppermute | solution.py:186
  27.1 10.0 %collective-permute-start.6 = (bf16[16,3072]{1,0:T(8,128)(2,1)S(1)}, bf16[16,3072]{1,0:T(8,128)(2,1)S(1)}, u32[]{:S(2)}, u32[]{:S(2)}) collective-permute-start(bf16[16,3072]{1,0:T(8,128)(2,1)S(1)} %get-tuple-element.17), channel_id=1, source_target_pairs={{0,16},{4,20},{8,24},{12,28},{16,0},{20,4},{24,8},{28,12},{1,17},{... | collective-permute-start | bytes 294920 | tf_op jit(solution)/shard_map/ppermute | solution.py:186
  27.1 10.0 %collective-permute-start.5 = (bf16[16,3072]{1,0:T(8,128)(2,1)S(1)}, bf16[16,3072]{1,0:T(8,128)(2,1)S(1)}, u32[]{:S(2)}, u32[]{:S(2)}) collective-permute-start(bf16[16,3072]{1,0:T(8,128)(2,1)S(1)} %get-tuple-element.18), channel_id=1, source_target_pairs={{0,8},{4,12},{8,0},{12,4},{16,24},{20,28},{24,16},{28,20},{1,9},{5... | collective-permute-start | bytes 294920 | tf_op jit(solution)/shard_map/ppermute | solution.py:186
  45.5 8.1 %copy-start.15 = (f32[16]{0:T(128)S(1)}, f32[16]{0:T(128)}, u32[]{:S(2)}) copy-start(f32[16]{0:T(128)} %param.37) | copy-start | bytes 196
  45.5 13.4 %copy-start.12 = (f32[4096]{0:T(1024)S(1)}, f32[4096]{0:T(1024)}, u32[]{:S(2)}) copy-start(f32[4096]{0:T(1024)} %param.31) | copy-start | bytes 49156
  50.1 6.4 %collective-permute-start.10 = (bf16[16,4096]{1,0:T(8,128)(2,1)S(1)}, bf16[16,4096]{1,0:T(8,128)(2,1)S(1)}, u32[]{:S(2)}, u32[]{:S(2)}) collective-permute-start(bf16[16,4096]{1,0:T(8,128)(2,1)S(1)} %convolution_convert_fusion.1), channel_id=1, source_target_pairs={{0,3},{1,2},{2,1},{3,0},{4,7},{5,6},{6,5},{7,4},{8,11},{9,10},{10,... | collective-permute-start | bytes 393224 | tf_op jit(solution)/shard_map/ppermute | solution.py:186
  52.6 6.0 %collective-permute-start.9 = (bf16[16,4096]{1,0:T(8,128)(2,1)S(1)}, bf16[16,4096]{1,0:T(8,128)(2,1)S(1)}, u32[]{:S(2)}, u32[]{:S(2)}) collective-permute-start(bf16[16,4096]{1,0:T(8,128)(2,1)S(1)} %convolution_convert_fusion.1), channel_id=1, source_target_pairs={{0,2},{1,3},{2,0},{3,1},{4,6},{5,7},{6,4},{7,5},{8,10},{9,11},{10,... | collective-permute-start | bytes 393224 | tf_op jit(solution)/shard_map/ppermute | solution.py:186
  53.1 5.6 %collective-permute-start.8 = (bf16[16,4096]{1,0:T(8,128)(2,1)S(1)}, bf16[16,4096]{1,0:T(8,128)(2,1)S(1)}, u32[]{:S(2)}, u32[]{:S(2)}) collective-permute-start(bf16[16,4096]{1,0:T(8,128)(2,1)S(1)} %convolution_convert_fusion.1), channel_id=1, source_target_pairs={{0,1},{1,0},{2,3},{3,2},{4,5},{5,4},{6,7},{7,6},{8,9},{9,8},{10,11... | collective-permute-start | bytes 393224 | tf_op jit(solution)/shard_map/ppermute | solution.py:186
  53.6 15.5 %copy-start.1 = (bf16[1,256,4096]{2,1,0:T(8,128)(2,1)S(1)}, bf16[1,256,4096]{2,1,0:T(8,128)(2,1)}, u32[]{:S(2)}) copy-start(bf16[1,256,4096]{2,1,0:T(8,128)(2,1)} %param.32) | copy-start | bytes 6291460
  59.3 10.6 %copy-start.2 = (bf16[1,256,4096]{2,1,0:T(8,128)(2,1)S(1)}, bf16[1,256,4096]{2,1,0:T(8,128)(2,1)}, u32[]{:S(2)}) copy-start(bf16[1,256,4096]{2,1,0:T(8,128)(2,1)} %param.33) | copy-start | bytes 6291460
  59.3 6.2 %collective-permute-start.13 = (bf16[8,4096]{1,0:T(8,128)(2,1)S(1)}, bf16[8,4096]{1,0:T(8,128)(2,1)S(1)}, u32[]{:S(2)}, u32[]{:S(2)}) collective-permute-start(bf16[8,4096]{1,0:T(8,128)(2,1)S(1)} %get-tuple-element.22), channel_id=1, source_target_pairs={{0,24},{4,28},{8,16},{12,20},{16,8},{20,12},{24,0},{28,4},{1,25},{... | collective-permute-start | bytes 196616 | tf_op jit(solution)/shard_map/ppermute | solution.py:186
  61.4 6.1 %collective-permute-start.12 = (bf16[8,4096]{1,0:T(8,128)(2,1)S(1)}, bf16[8,4096]{1,0:T(8,128)(2,1)S(1)}, u32[]{:S(2)}, u32[]{:S(2)}) collective-permute-start(bf16[8,4096]{1,0:T(8,128)(2,1)S(1)} %get-tuple-element.23), channel_id=1, source_target_pairs={{0,16},{4,20},{8,24},{12,28},{16,0},{20,4},{24,8},{28,12},{1,17},{... | collective-permute-start | bytes 196616 | tf_op jit(solution)/shard_map/ppermute | solution.py:186
  61.4 6.1 %collective-permute-start.11 = (bf16[8,4096]{1,0:T(8,128)(2,1)S(1)}, bf16[8,4096]{1,0:T(8,128)(2,1)S(1)}, u32[]{:S(2)}, u32[]{:S(2)}) collective-permute-start(bf16[8,4096]{1,0:T(8,128)(2,1)S(1)} %get-tuple-element.24), channel_id=1, source_target_pairs={{0,8},{4,12},{8,0},{12,4},{16,24},{20,28},{24,16},{28,20},{1,9},{5... | collective-permute-start | bytes 196616 | tf_op jit(solution)/shard_map/ppermute | solution.py:186
  67.5 1.6 %collective-permute-start.14 = (bf16[32,4096]{1,0:T(8,128)(2,1)S(1)}, bf16[32,4096]{1,0:T(8,128)(2,1)S(1)}, u32[]{:S(2)}, u32[]{:S(2)}) collective-permute-start(bf16[32,4096]{1,0:T(8,128)(2,1)S(1)} %pad_maximum_fusion), channel_id=1, source_target_pairs={{0,4},{4,0},{8,12},{12,8},{16,20},{20,16},{24,28},{28,24},{1,5},{5... | collective-permute-start | bytes 786440 | tf_op jit(solution)/shard_map/ppermute | solution.py:186
  70.7 14.3 %collective-permute-start.17 = (bf16[64,256]{1,0:T(8,128)(2,1)S(1)}, bf16[64,256]{1,0:T(8,128)(2,1)S(1)}, u32[]{:S(2)}, u32[]{:S(2)}) collective-permute-start(bf16[64,256]{1,0:T(8,128)(2,1)S(1)} %multiply_convert_fusion), channel_id=1, source_target_pairs={{0,3},{1,2},{2,1},{3,0},{4,7},{5,6},{6,5},{7,4},{8,11},{9,10},{10,... | collective-permute-start | bytes 98312 | tf_op jit(solution)/shard_map/ppermute | solution.py:186
  72.3 12.6 %collective-permute-start.16 = (bf16[64,256]{1,0:T(8,128)(2,1)S(1)}, bf16[64,256]{1,0:T(8,128)(2,1)S(1)}, u32[]{:S(2)}, u32[]{:S(2)}) collective-permute-start(bf16[64,256]{1,0:T(8,128)(2,1)S(1)} %multiply_convert_fusion), channel_id=1, source_target_pairs={{0,2},{1,3},{2,0},{3,1},{4,6},{5,7},{6,4},{7,5},{8,10},{9,11},{10,... | collective-permute-start | bytes 98312 | tf_op jit(solution)/shard_map/ppermute | solution.py:186
  73.7 11.3 %collective-permute-start.15 = (bf16[64,256]{1,0:T(8,128)(2,1)S(1)}, bf16[64,256]{1,0:T(8,128)(2,1)S(1)}, u32[]{:S(2)}, u32[]{:S(2)}) collective-permute-start(bf16[64,256]{1,0:T(8,128)(2,1)S(1)} %multiply_convert_fusion), channel_id=1, source_target_pairs={{0,1},{1,0},{2,3},{3,2},{4,5},{5,4},{6,7},{7,6},{8,9},{9,8},{10,11... | collective-permute-start | bytes 98312 | tf_op jit(solution)/shard_map/ppermute | solution.py:186
  85.6 1.3 %collective-permute-start.18 = (bf16[32,1024]{1,0:T(8,128)(2,1)S(1)}, bf16[32,1024]{1,0:T(8,128)(2,1)S(1)}, u32[]{:S(2)}, u32[]{:S(2)}) collective-permute-start(bf16[32,1024]{1,0:T(8,128)(2,1)S(1)} %slice.94), channel_id=1, source_target_pairs={{0,4},{4,0},{8,12},{12,8},{16,20},{20,16},{24,28},{28,24},{1,5},{5... | collective-permute-start | bytes 196616 | tf_op jit(solution)/shard_map/ppermute | solution.py:186
  86.9 4.5 %collective-permute-start.19 = (bf16[16,1024]{1,0:T(8,128)(2,1)S(1)}, bf16[16,1024]{1,0:T(8,128)(2,1)S(1)}, u32[]{:S(2)}, u32[]{:S(2)}) collective-permute-start(bf16[16,1024]{1,0:T(8,128)(2,1)S(1)} %pad_maximum_fusion.7), channel_id=1, source_target_pairs={{0,8},{4,12},{8,0},{12,4},{16,24},{20,28},{24,16},{28,20},{1,9},{5... | collective-permute-start | bytes 98312 | tf_op jit(solution)/shard_map/ppermute | solution.py:186
  87.6 5.1 %collective-permute-start.20 = (bf16[16,1024]{1,0:T(8,128)(2,1)S(1)}, bf16[16,1024]{1,0:T(8,128)(2,1)S(1)}, u32[]{:S(2)}, u32[]{:S(2)}) collective-permute-start(bf16[16,1024]{1,0:T(8,128)(2,1)S(1)} %pad_maximum_fusion.8), channel_id=1, source_target_pairs={{0,16},{4,20},{8,24},{12,28},{16,0},{20,4},{24,8},{28,12},{1,17},{... | collective-permute-start | bytes 98312 | tf_op jit(solution)/shard_map/ppermute | solution.py:186
  90.3 5.7 %collective-permute-start.21 = (bf16[16,1024]{1,0:T(8,128)(2,1)S(1)}, bf16[16,1024]{1,0:T(8,128)(2,1)S(1)}, u32[]{:S(2)}, u32[]{:S(2)}) collective-permute-start(bf16[16,1024]{1,0:T(8,128)(2,1)S(1)} %pad_maximum_fusion.9), channel_id=1, source_target_pairs={{0,24},{4,28},{8,16},{12,20},{16,8},{20,12},{24,0},{28,4},{1,25},{... | collective-permute-start | bytes 98312 | tf_op jit(solution)/shard_map/ppermute | solution.py:186
  (6 other events, 12.1 us)

commit v2 on v1

--- a/solution.py
+++ b/solution.py
@@ -186,13 +186,18 @@
     return lax.ppermute(x, axis, [(k, k ^ offset) for k in range(size)])
 
 
-def project_kernel(tp_ref, *refs):
+IN_VMEM = pl.BlockSpec(memory_space=pltpu.VMEM)
+
+
+def small_kernel(**more):
+    return pltpu.CompilerParams(vmem_limit_bytes=8 * 2**20, **more)
+
+
+def project_kernel(*refs):
     piece_count = len(refs) - 7
     pieces = refs[:piece_count]
     gain, wq, wk, wv, wg, keep, send = refs[piece_count:]
     rows = pieces[0].shape[0] // CORES
-    width = wq.shape[1]
-    span = wv.shape[1]
     scaled = [bf16(f32(p[...]) * gain[...]) for p in pieces]
     x = jnp.concatenate(
         [p[:rows] for p in scaled] + [p[rows:] for p in scaled], axis=0
@@ -206,33 +211,17 @@
         start += w.shape[1]
 
 
-def project(tp_index, pieces, gain, wq, wk, wv, wg):
-    heads = wv.shape[1] // DV
-    features = wq.shape[0]
+def project(pieces, gain, wq, wk, wv, wg):
     rows = pieces[0].shape[0] * len(pieces) // CORES
-    head_span = 2 * KEY_CHANNELS + 2 * DV
-    own = lambda j, t: (0, t[0] * heads + j)
-    local = lambda j, t: (0, j)
-    whole = lambda j, t: (0, 0)
-    out = jax.ShapeDtypeStruct((rows, heads * head_span), jnp.bfloat16)
+    out = jax.ShapeDtypeStruct((rows, 2 * (wq.shape[1] + wv.shape[1])), jnp.bfloat16)
     return pl.pallas_call(
         project_kernel,
-        grid_spec=pltpu.PrefetchScalarGridSpec(
-            num_scalar_prefetch=1,
-            grid=(heads,),
-            in_specs=[pl.BlockSpec(p.shape, whole) for p in pieces]
-            + [
-                pl.BlockSpec((1, features), whole),
-                pl.BlockSpec((features, KEY_CHANNELS), own),
-                pl.BlockSpec((features, KEY_CHANNELS), own),
-                pl.BlockSpec((features, DV), local),
-                pl.BlockSpec((features, DV), local),
-            ],
-            out_specs=[pl.BlockSpec((rows, head_span), local)] * 2,
-        ),
+        in_specs=[IN_VMEM] * (len(pieces) + 5),
+        out_specs=[IN_VMEM] * 2,
         out_shape=[out, out],
+        compiler_params=small_kernel(),
         name="project",
-    )(tp_index.reshape(1), *pieces, gain.reshape(1, features), wq, wk, wv, wg)
+    )(*pieces, gain.reshape(1, -1), wq, wk, wv, wg)
 
 
 def as_columns(row, heads):
@@ -242,72 +231,66 @@
 
 
 def readout_kernel(*refs):
-    piece_count = len(refs) - 12
+    piece_count = len(refs) - 13
     pieces = refs[:piece_count]
-    (row_scale, decay, head_gain, state, gated, key_out, value_out, qd, qk, gate, read, _) = refs[
-        piece_count:
+    (row_scale, decay, head_gain, state, w_out, partial, key_out, value_out) = refs[
+        piece_count : piece_count + 8
     ]
-    step = pl.program_id(0)
-    heads = value_out.shape[1] // DV
-    head_span = 2 * KEY_CHANNELS + 2 * DV
-    per_step = state.shape[0]
-
-    @pl.when(step == 0)
-    def _():
-        for h in range(heads):
-            base = h * head_span
-            total = f32(pieces[0][:, base : base + head_span])
-            for p in pieces[1:]:
-                total = total + f32(p[:, base : base + head_span])
-            total = total * row_scale[...]
-            q = f32(bf16(total[:, :KEY_CHANNELS] * KEY_CHANNELS ** (-0.5)))
-            k = f32(bf16(total[:, KEY_CHANNELS : 2 * KEY_CHANNELS]))
-            v = f32(bf16(total[:, 2 * KEY_CHANNELS : 2 * KEY_CHANNELS + DV]))
-            g = f32(bf16(total[:, 2 * KEY_CHANNELS + DV :]))
-            ks = slice(h * KEY_CHANNELS, (h + 1) * KEY_CHANNELS)
-            vs = slice(h * DV, (h + 1) * DV)
-            key_out[:, ks] = k
-            value_out[:, vs] = v
-            qd[:, ks] = q * decay[:, ks]
-            qk[:, vs] = jnp.sum(q * k, axis=-1, keepdims=True) * v
-            gate[:, vs] = g / (1.0 + jnp.exp(-g))
-
-    for j in range(per_step):
-        s = step * per_step + j
+    qd, qk, gate, read, gated = refs[piece_count + 8 :]
+    seqs, values = value_out.shape
+    heads = values // DV
+    keys = key_out.shape[1]
+
+    def summed(start, width):
+        total = f32(pieces[0][:, start : start + width])
+        for p in pieces[1:]:
+            total = total + f32(p[:, start : start + width])
+        return total * row_scale[...]
+
+    for h in range(heads):
+        ks = slice(h * KEY_CHANNELS, (h + 1) * KEY_CHANNELS)
+        vs = slice(h * DV, (h + 1) * DV)
+        q = f32(bf16(summed(h * KEY_CHANNELS, KEY_CHANNELS) * KEY_CHANNELS ** (-0.5)))
+        k = f32(bf16(summed(keys + h * KEY_CHANNELS, KEY_CHANNELS)))
+        v = f32(bf16(summed(2 * keys + h * DV, DV)))
+        g = f32(bf16(summed(2 * keys + values + h * DV, DV)))
+        key_out[:, ks] = k
+        value_out[:, vs] = v
+        qd[:, ks] = q * decay[:, ks]
+        qk[:, vs] = jnp.sum(q * k, axis=-1, keepdims=True) * v
+        gate[:, vs] = g / (1.0 + jnp.exp(-g))
+
+    def body(s, carry):
         cols = as_columns(qd[pl.ds(s, 1), :], heads)
         for h in range(heads):
             vs = slice(h * DV, (h + 1) * DV)
-            prod = cols[:, h : h + 1] * state[j, :, vs]
-            read[pl.ds(s, 1), vs] = jnp.sum(prod, axis=0, keepdims=True)
-
-    @pl.when(step == pl.num_programs(0) - 1)
-    def _():
-        for h in range(heads):
-            vs = slice(h * DV, (h + 1) * DV)
-            r = read[:, vs] + qk[:, vs]
-            inv = lax.rsqrt(jnp.mean(r * r, axis=-1, keepdims=True) + epsilon)
-            gated[:, vs] = bf16(r * inv * head_gain[...] * gate[:, vs])
-
-
-def readout_call(pieces, row_scale, decay, head_gain, state):
+            col = cols[:, h : h + 1]
+            acc = jnp.zeros((8, DV), jnp.float32)
+            for i in range(0, KEY_CHANNELS, 8):
+                acc = acc + col[i : i + 8] * state[s, i : i + 8, vs]
+            read[pl.ds(s, 1), vs] = jnp.sum(acc, axis=0, keepdims=True)
+        return carry
+
+    lax.fori_loop(0, seqs, body, 0, unroll=4)
+    for h in range(heads):
+        vs = slice(h * DV, (h + 1) * DV)
+        r = read[:, vs] + qk[:, vs]
+        inv = lax.rsqrt(jnp.mean(r * r, axis=-1, keepdims=True) + epsilon)
+        gated[:, vs] = bf16(r * inv * head_gain[...] * gate[:, vs])
+    partial[...] = bf16(
+        jnp.dot(gated[...], w_out[...], preferred_element_type=jnp.float32)
+    )
+
+
+def readout_call(pieces, row_scale, decay, head_gain, state, w_out):
     seqs, channels, values = state.shape
     keys = decay.shape[1]
-    per_step = 2
-    whole = lambda i: (0, 0)
-    full = lambda a: pl.BlockSpec(a.shape, whole)
     return pl.pallas_call(
         readout_kernel,
-        grid=(seqs // per_step,),
-        in_specs=[full(p) for p in pieces]
-        + [full(row_scale), full(decay), full(head_gain)]
-        + [pl.BlockSpec((per_step, channels, values), lambda i: (i, 0, 0))],
-        out_specs=[
-            pl.BlockSpec((seqs, values), whole),
-            pl.BlockSpec((seqs, keys), whole),
-            pl.BlockSpec((seqs, values), whole),
-        ],
+        in_specs=[IN_VMEM] * (len(pieces) + 5),
+        out_specs=[IN_VMEM] * 3,
         out_shape=[
-            jax.ShapeDtypeStruct((seqs, values), jnp.bfloat16),
+            jax.ShapeDtypeStruct((seqs, w_out.shape[1]), jnp.bfloat16),
             jax.ShapeDtypeStruct((seqs, keys), jnp.float32),
             jax.ShapeDtypeStruct((seqs, values), jnp.float32),
         ],
@@ -316,45 +299,49 @@
             pltpu.VMEM((seqs, values), jnp.float32),
             pltpu.VMEM((seqs, values), jnp.float32),
             pltpu.VMEM((seqs, values), jnp.float32),
-            pltpu.VMEM((8, 128), jnp.float32),
+            pltpu.VMEM((seqs, values), jnp.bfloat16),
         ],
+        compiler_params=small_kernel(),
         name="readout",
-    )(*pieces, row_scale, decay, head_gain, state)
-
-
-def state_kernel(decay, keys, values, state, out):
-    step = pl.program_id(0)
-    per_step = state.shape[0]
+    )(*pieces, row_scale, decay, head_gain, state, w_out)
+
+
+def state_kernel(first, decay, keys, values, state, *rest):
+    out = rest[-1]
+    s = first + pl.program_id(0)
     heads = values.shape[1] // DV
-    for j in range(per_step):
-        s = step * per_step + j
-        decay_cols = as_columns(decay[pl.ds(s, 1), :], heads)
-        key_cols = as_columns(keys[pl.ds(s, 1), :], heads)
-        value_row = values[pl.ds(s, 1), :]
-        for h in range(heads):
-            vs = slice(h * DV, (h + 1) * DV)
-            out[j, :, vs] = (
-                decay_cols[:, h : h + 1] * state[j, :, vs]
-                + key_cols[:, h : h + 1] * value_row[:, vs]
-            )
-
-
-def state_call(decay, keys, values, state):
+    decay_cols = as_columns(decay[pl.ds(s, 1), :], heads)
+    key_cols = as_columns(keys[pl.ds(s, 1), :], heads)
+    value_row = values[pl.ds(s, 1), :]
+    for h in range(heads):
+        vs = slice(h * DV, (h + 1) * DV)
+        out[0, :, vs] = (
+            decay_cols[:, h : h + 1] * state[0, :, vs]
+            + key_cols[:, h : h + 1] * value_row[:, vs]
+        )
+
+
+def state_call(first, count, decay, keys, values, state, earlier):
     seqs, channels, width = state.shape
-    per_step = 2
-    block = pl.BlockSpec((per_step, channels, width), lambda i: (i, 0, 0))
+    block = pl.BlockSpec((1, channels, width), lambda i: (first + i, 0, 0))
     full = lambda a: pl.BlockSpec(a.shape, lambda i: (0, 0))
+    kept = () if earlier is None else (earlier,)
     return pl.pallas_call(
-        state_kernel,
-        grid=(seqs // per_step,),
-        in_specs=[full(decay), full(keys), full(values), block],
+        lambda *refs: state_kernel(first, *refs),
+        grid=(count,),
+        in_specs=[full(decay), full(keys), full(values), block]
+        + [pl.BlockSpec(memory_space=pl.ANY)] * len(kept),
         out_specs=block,
         out_shape=jax.ShapeDtypeStruct(state.shape, jnp.float32),
+        input_output_aliases={4: 0} if kept else {},
+        compiler_params=small_kernel(),
         cost_estimate=pl.CostEstimate(
-            flops=40 * state.size, bytes_accessed=8 * state.size, transcendentals=0
+            flops=40 * count * channels * width,
+            bytes_accessed=8 * count * channels * width,
+            transcendentals=0,
         ),
         name="state_update",
-    )(decay, keys, values, state)
+    )(decay, keys, values, pltpu.with_memory_space_constraint(state, pltpu.HBM), *kept)
 
 
 def on_device_paired(
@@ -392,16 +379,18 @@
     features = query_matrix.shape[0]
 
     partner_stream = exchange(stream, "ep", 1)
-    pieces = []
+    blocks = []
     for d in range(chips):
         start = ((chip ^ d) * CORES + core) * features
         both = [lax.dynamic_slice_in_dim(a, start, features, 1) for a in (stream, partner_stream)]
-        block = jnp.concatenate(both, axis=0)
-        pieces.append(exchange(block, "ep", CORES * d) if d else block)
+        blocks.append(jnp.concatenate(both, axis=0))
+    pieces = [exchange(block, "ep", CORES * d) if d else block for d, block in enumerate(blocks)]
     own_gain = lax.dynamic_slice_in_dim(mixer_norm_gain, ep_index * features, features, 0)
-    keep, send = project(
-        tp_index, pieces, own_gain, query_matrix, key_matrix, value_matrix, output_gate_weight
-    )
+    own_query, own_key = [
+        lax.dynamic_slice_in_dim(w, first_key, key_column_span, 1)
+        for w in (query_matrix, key_matrix)
+    ]
+    keep, send = project(pieces, own_gain, own_query, own_key, value_matrix, output_gate_weight)
     on_chip = bf16(f32(keep) + f32(exchange(send, "ep", 1)))
     sums = []
     for d in range(chips):
@@ -417,14 +406,21 @@
     boost = lax.dynamic_slice_in_dim(forgetting_boost, first_key, key_column_span, 1)
     decay = jnp.exp(jax.nn.log_sigmoid(logit) / forgetting_softness - boost)
 
-    gated_rows, key_rows, value_rows = readout_call(
-        sums, row_scale, decay, head_norm_gain.reshape(1, DV), previous_state
-    )
-    partial_out = bf16(jnp.dot(gated_rows, output_matrix, preferred_element_type=jnp.float32))
+    partial_out, key_rows, value_rows = readout_call(
+        sums, row_scale, decay, head_norm_gain.reshape(1, DV), previous_state, output_matrix
+    )
+    bounds = [seq_count * n // 16 for n in (0, 5, 9, 12, 16)]
+
+    def update(n, earlier, after):
+        held, _ = lax.optimization_barrier((decay, after))
+        return state_call(
+            bounds[n], bounds[n + 1] - bounds[n], held, key_rows, value_rows, previous_state, earlier
+        )
+
     mixed = floats + f32(partial_out)
     for d in range(1, tp_count):
         mixed = mixed + f32(exchange(partial_out, "tp", d))
-    new_state = state_call(decay, key_rows, value_rows, previous_state)
+    new_state = update(0, None, partial_out)
     mixed = bf16(mixed)
     normed_two = rms_scaled(mixed, mixture_norm_gain)
 
@@ -460,6 +456,8 @@
             "sc,sd->cd", bf16(placing), normed_two, preferred_element_type=jnp.float32
         )
     )
+    outgoing, new_state = lax.optimization_barrier((outgoing, new_state))
+    new_state = update(1, new_state, outgoing)
     arrived = []
     for d in range(chips):
         block = outgoing[d * capacity : (d + 1) * capacity]
@@ -475,6 +473,8 @@
         rows, expert_up_weight[0], contract_last, preferred_element_type=jnp.float32
     )
     hidden = bf16(jax.nn.silu(gate_pre) * up_pre)
+    hidden, new_state = lax.optimization_barrier((hidden, new_state))
+    new_state = update(2, new_state, hidden)
     parts = jnp.stack([hidden] + [exchange(hidden, "tp", d) for d in range(1, tp_count)])
     hidden_all = jnp.concatenate(
         [
@@ -486,9 +486,12 @@
     outputs = bf16(
         jnp.dot(hidden_all, expert_down_weight[0], preferred_element_type=jnp.float32)
     )
+    outputs, new_state = lax.optimization_barrier((outputs, new_state))
     width_local = outputs.shape[1]
     same_core = outputs[:slot_count].reshape(chips, capacity, width_local)
-    other_core = exchange(outputs[slot_count:], "ep", 1).reshape(chips, capacity, width_local)
+    other_core = exchange(outputs[slot_count:], "ep", 1)
+    new_state = update(3, new_state, other_core)
+    other_core = other_core.reshape(chips, capacity, width_local)
     back = []
     for d in range(chips):
         block = jnp.concatenate([same_core[d], other_core[d]], axis=0)

time: 97.6 us -> 85.2 us (0.87)
  waiting for transfers between devices: 27.2 us -> 15.2 us
  local copies, waits for them, and re-layouts: 4.91 us -> 9.96 us
  matrix products: 9.77 us -> 4.78 us
  other arithmetic: 4.81 us -> 3.66 us
    ppermute x22, waiting for transfers between devices: 27.2 us -> 15.2 us  [exchange(): return lax.ppermute(x, axis, [(k, k ^ offset) for k in range(size)])]
    unnamed x37 -> x31, local copies, waits for them, and re-layouts: 1.34 us -> 6.84 us
    dot_general x1 -> x0, matrix products: 4.62 us -> none  [on_device_paired(): jnp.dot(gated_rows, output_matrix, preferred_element_type=jnp.float32)]
    dynamic_slice x0 -> x1, local copies, waits for them, and re-layouts: none -> 1.27 us  [on_device_paired(): lax.dynamic_slice_in_dim(w, first_key, key_column_span, 1)]
    convert_element_type x1, other arithmetic: 1.09 us -> 0.09 us  [bf16(): return x.astype(jnp.bfloat16)]
    pallas_call x3 -> x6, Pallas kernels: 22.8 us -> 23.4 us  [the longest x4 18.5 us: state_call(): pl.pallas_call(lambda *refs: state_kernel(first, *refs), grid=(count,), i...]
  transfers between devices with their start and end apart: 22 -> 22, of which waited for: 13 -> 7; matrix products, arithmetic and copies ran while one was open for 9% -> 9% of each run, Pallas kernels for 11% -> 22%
where the time goes in v2:
time: 85.2 us; the launch traced here: 84.6 us
  starting transfers between devices  26.6 us (31%)
  Pallas kernels  23.4 us (27%)
  waiting for transfers between devices  15.2 us (18%)
  local copies, waits for them, and re-layouts  9.96 us (12%)
  matrix products  4.78 us (6%)
  other arithmetic  3.66 us (4%)
  between operations  0.98 us (1%)
    ppermute x22, starting transfers between devices, exchange(): return lax.ppermute(x, axis, [(k, k ^ offset) for k in range(size)])  26.6 us
    pallas_call x4, Pallas kernels, state_call(): pl.pallas_call(lambda *refs: state_kernel(first, *refs), grid=(count,), i...  18.5 us
    ppermute x22, waiting for transfers between devices, exchange(): return lax.ppermute(x, axis, [(k, k ^ offset) for k in range(size)])  15.2 us
    unnamed x31, local copies, waits for them, and re-layouts  6.84 us
    pallas_call x1, Pallas kernels, readout_call(): pl.pallas_call(readout_kernel, in_specs=[IN_VMEM] * (len(pieces) + 5), ou...  3.61 us
  transfers between devices with their start and end apart: 22, of which 7 were waited for; matrix products, arithmetic and copies ran while one was open for 9% of the time, Pallas kernels for 22%

profile of v2, /device:TPU:0, one launch (start us, length us, event | category | flops | bytes accessed | tf_op | source)
XLA Modules:
  0.0 84.6 jit_solution(9732538132736378054)
XLA Ops:
  1.2 1.0 %fusion.12 = f32[16]{0:T(128)S(1)} fusion(bf16[16,4096]{1,0:T(8,128)(2,1)} %param.19), kind=kLoop, calls=%fused_computation.19 | loop fusion | flops 196592 | bytes 131136 | tf_op jit(solution)/shard_map/reduce_sum | solution.py:401
  4.2 0.8 dynamic_slice.63
  5.2 0.9 %constant_dynamic-slice_fusion.3 = (bf16[16,512]{1,0:T(8,128)(2,1)S(1)}, bf16[16,512]{1,0:T(8,128)(2,1)S(1)}, bf16[16,512]{1,0:T(8,128)(2,1)S(1)}, bf16[16,512]{1,0:T(8,128)(2,1)S(1)}) fusion(bf16[16,4096]{1,0:T(8,128)(2,1)} %param.19, s32[]{:T(128)S(6)} %select_n.109, s32[]{:T(128)S(6)} %select_n.107, s32[]{:T(128)S(6)} %select_n.106, s32[]{:T(128)S(6)} %select_n.108), kind=kLoop, calls=%fused_computation.79 | loop fusion | bytes 131088 | tf_op jit(solution)/shard_map/dynamic_slice | solution.py:385
  6.1 1.3 %constant_dynamic-slice_fusion = (bf16[512,512]{1,0:T(8,128)(2,1)S(1)}, bf16[512,512]{1,0:T(8,128)(2,1)S(1)}) fusion(bf16[512,2048]{1,0:T(8,128)(2,1)} %param.23, s32[]{:T(128)S(6)} %select_n.111, bf16[512,2048]{1,0:T(8,128)(2,1)} %param.22), kind=kLoop, calls=%fused_computation.76 | loop fusion | bytes 2097156 | tf_op jit(solution)/shard_map/dynamic_slice | solution.py:390
  7.4 2.9 %collective-permute-start.1 = (bf16[32,512]{1,0:T(8,128)(2,1)S(1)}, bf16[32,512]{1,0:T(8,128)(2,1)S(1)}, u32[]{:S(2)}, u32[]{:S(2)}) collective-permute-start(bf16[32,512]{1,0:T(8,128)(2,1)S(1)} %pad_maximum_fusion.3), channel_id=1, source_target_pairs={{0,8},{4,12},{8,0},{12,4},{16,24},{20,28},{24,16},{28,20},{1,9},{5... | collective-permute-start | bytes 98312 | tf_op jit(solution)/shard_map/ppermute | solution.py:186
  10.3 2.6 %collective-permute-start.2 = (bf16[32,512]{1,0:T(8,128)(2,1)S(1)}, bf16[32,512]{1,0:T(8,128)(2,1)S(1)}, u32[]{:S(2)}, u32[]{:S(2)}) collective-permute-start(bf16[32,512]{1,0:T(8,128)(2,1)S(1)} %pad_maximum_fusion.4), channel_id=1, source_target_pairs={{0,16},{4,20},{8,24},{12,28},{16,0},{20,4},{24,8},{28,12},{1,17},{... | collective-permute-start | bytes 98312 | tf_op jit(solution)/shard_map/ppermute | solution.py:186
  12.9 2.8 %collective-permute-done.2.refs_2_ = bf16[32,512]{1,0:T(8,128)(2,1)S(1)} collective-permute-done((bf16[32,512]{1,0:T(8,128)(2,1)S(1)}, bf16[32,512]{1,0:T(8,128)(2,1)S(1)}, u32[]{:S(2)}, u32[]{:S(2)}) %collective-permute-start.2) | collective-permute-done | bytes 32800 | tf_op jit(solution)/shard_map/ppermute | solution.py:186
  15.7 2.9 %collective-permute-done.3.refs_3_ = bf16[32,512]{1,0:T(8,128)(2,1)S(1)} collective-permute-done((bf16[32,512]{1,0:T(8,128)(2,1)S(1)}, bf16[32,512]{1,0:T(8,128)(2,1)S(1)}, u32[]{:S(2)}, u32[]{:S(2)}) %collective-permute-start.3) | collective-permute-done | bytes 32800 | tf_op jit(solution)/shard_map/ppermute | solution.py:186
  18.6 1.3 %project.1 = (bf16[64,3072]{1,0:T(8,128)(2,1)S(1)}, bf16[64,3072]{1,0:T(8,128)(2,1)}) custom-call(bf16[32,512]{1,0:T(8,128)(2,1)S(1)} %pad_maximum_fusion.2.refs_0_, bf16[32,512]{1,0:T(8,128)(2,1)S(1)} %collective-permute-done.1.refs_1_, bf16[32,512]{1,0:T(8,128)(2,1)S(1)} %collective-permute-done.2.refs_2_, ...), custom_call_target="tpu_custom_call" | custom-call | tf_op jit(solution)/shard_map/project/pallas_call | solution.py:217
  20.0 1.6 %fusion.39.refs_5_.refs_0_ = f32[16,512]{1,0:T(8,128)S(1)} fusion(f32[16,2048]{1,0:T(8,128)} %param.28, s32[]{:T(128)S(6)} %select_n.111, bf16[64,2048]{1,0:T(8,128)(2,1)} %param.27, bf16[4096,64]{0,1:T(8,128)(2,1)} %param.26, bf16[16,4096]{1,0:T(8,128)(2,1)} %param.19, f32[4096]{0:T(1024)} %param.21, f32[16]{0:T(128)} %get-tuple-element.67), kind=kOutput, calls=%fused_computation.46 | convolution fusion | flops 9782272 | bytes 804352 | tf_op jit(solution)/shard_map/dot_general | solution.py:405
  22.1 0.9 %collective-permute-start.6 = (bf16[16,3072]{1,0:T(8,128)(2,1)S(1)}, bf16[16,3072]{1,0:T(8,128)(2,1)S(1)}, u32[]{:S(2)}, u32[]{:S(2)}) collective-permute-start(bf16[16,3072]{1,0:T(8,128)(2,1)S(1)} %get-tuple-element.37), channel_id=1, source_target_pairs={{0,16},{4,20},{8,24},{12,28},{16,0},{20,4},{24,8},{28,12},{1,17},{... | collective-permute-start | bytes 294920 | tf_op jit(solution)/shard_map/ppermute | solution.py:186
  23.0 3.4 %collective-permute-start.7 = (bf16[16,3072]{1,0:T(8,128)(2,1)S(1)}, bf16[16,3072]{1,0:T(8,128)(2,1)S(1)}, u32[]{:S(2)}, u32[]{:S(2)}) collective-permute-start(bf16[16,3072]{1,0:T(8,128)(2,1)S(1)} %get-tuple-element.36), channel_id=1, source_target_pairs={{0,24},{4,28},{8,16},{12,20},{16,8},{20,12},{24,0},{28,4},{1,25},{... | collective-permute-start | bytes 294920 | tf_op jit(solution)/shard_map/ppermute | solution.py:186
  26.5 1.6 %collective-permute-done.5.refs_1_ = bf16[16,3072]{1,0:T(8,128)(2,1)S(1)} collective-permute-done((bf16[16,3072]{1,0:T(8,128)(2,1)S(1)}, bf16[16,3072]{1,0:T(8,128)(2,1)S(1)}, u32[]{:S(2)}, u32[]{:S(2)}) %collective-permute-start.5) | collective-permute-done | bytes 98336 | tf_op jit(solution)/shard_map/ppermute | solution.py:186
  28.1 4.9 %collective-permute-done.6.refs_2_ = bf16[16,3072]{1,0:T(8,128)(2,1)S(1)} collective-permute-done((bf16[16,3072]{1,0:T(8,128)(2,1)S(1)}, bf16[16,3072]{1,0:T(8,128)(2,1)S(1)}, u32[]{:S(2)}, u32[]{:S(2)}) %collective-permute-start.6) | collective-permute-done | bytes 98336 | tf_op jit(solution)/shard_map/ppermute | solution.py:186
  33.0 3.4 %copy-done.1 = f32[16,128,1024]{2,1,0:T(8,128)S(1)} copy-done((f32[16,128,1024]{2,1,0:T(8,128)S(1)}, f32[16,128,1024]{2,1,0:T(8,128)}, u32[]{:S(2)}) %copy-start.1) | copy-done | bytes 8388632
  36.4 3.4 %copy-done.2 = bf16[1024,4096]{1,0:T(8,128)(2,1)S(1)} copy-done((bf16[1024,4096]{1,0:T(8,128)(2,1)S(1)}, bf16[1024,4096]{1,0:T(8,128)(2,1)}, u32[]{:S(2)}) %copy-start.2) | copy-done | bytes 8388632
  39.8 3.6 %readout.1 = (bf16[16,4096]{1,0:T(8,128)(2,1)S(1)}, f32[16,512]{1,0:T(8,128)S(1)}, f32[16,1024]{1,0:T(8,128)S(1)}) custom-call(bf16[16,3072]{1,0:T(8,128)(2,1)S(1)} %get-tuple-element.39.refs_0_, bf16[16,3072]{1,0:T(8,128)(2,1)S(1)} %collective-permute-done.5.refs_1_, bf16[16,3072]{1,0:T(8,128)(2,1)S(1)} %collective-permute-done.6.refs_2_, ...), custom_call_target="tpu_custom_call" | custom-call | tf_op jit(solution)/shard_map/readout/pallas_call | solution.py:288
  43.4 2.5 %collective-permute-start.10 = (bf16[16,4096]{1,0:T(8,128)(2,1)S(1)}, bf16[16,4096]{1,0:T(8,128)(2,1)S(1)}, u32[]{:S(2)}, u32[]{:S(2)}) collective-permute-start(bf16[16,4096]{1,0:T(8,128)(2,1)S(1)} %get-tuple-element.19), channel_id=1, source_target_pairs={{0,3},{1,2},{2,1},{3,0},{4,7},{5,6},{6,5},{7,4},{8,11},{9,10},{10,... | collective-permute-start | bytes 393224 | tf_op jit(solution)/shard_map/ppermute | solution.py:186
  46.9 5.5 %state_update.4.refs_4_ = f32[16,128,1024]{2,1,0:T(8,128)} custom-call(f32[16,512]{1,0:T(8,128)S(1)} %fusion.39.refs_5_.refs_0_, f32[16,512]{1,0:T(8,128)S(1)} %get-tuple-element.21.refs_1_, f32[16,1024]{1,0:T(8,128)S(1)} %get-tuple-element.22.refs_2_, f32[16,128,1024]{2,1,0:T(8,128)} %refs_3_.7), custom_call_target="tpu_custom_call" | custom-call | flops 26214400 | bytes 5242880 | tf_op jit(solution)/shard_map/state_update/pallas_call | solution.py:329
  53.1 2.0 %collective-permute-start.11 = (bf16[8,4096]{1,0:T(8,128)(2,1)S(1)}, bf16[8,4096]{1,0:T(8,128)(2,1)S(1)}, u32[]{:S(2)}, u32[]{:S(2)}) collective-permute-start(bf16[8,4096]{1,0:T(8,128)(2,1)S(1)} %get-tuple-element.44), channel_id=1, source_target_pairs={{0,8},{4,12},{8,0},{12,4},{16,24},{20,28},{24,16},{28,20},{1,9},{5... | collective-permute-start | bytes 196616 | tf_op jit(solution)/shard_map/ppermute | solution.py:186
  55.1 2.4 %collective-permute-start.13 = (bf16[8,4096]{1,0:T(8,128)(2,1)S(1)}, bf16[8,4096]{1,0:T(8,128)(2,1)S(1)}, u32[]{:S(2)}, u32[]{:S(2)}) collective-permute-start(bf16[8,4096]{1,0:T(8,128)(2,1)S(1)} %get-tuple-element.42), channel_id=1, source_target_pairs={{0,24},{4,28},{8,16},{12,20},{16,8},{20,12},{24,0},{28,4},{1,25},{... | collective-permute-start | bytes 196616 | tf_op jit(solution)/shard_map/ppermute | solution.py:186
  57.6 4.6 %state_update.5.refs_4_ = f32[16,128,1024]{2,1,0:T(8,128)} custom-call(f32[16,512]{1,0:T(8,128)S(1)} %fusion.39.refs_5_.refs_0_, f32[16,512]{1,0:T(8,128)S(1)} %get-tuple-element.21.refs_1_, f32[16,1024]{1,0:T(8,128)S(1)} %get-tuple-element.22.refs_2_, f32[16,128,1024]{2,1,0:T(8,128)} %refs_3_.7, ...), custom_call_target="tpu_custom_call", output_to_operand_aliasing={{}: (4, {})} | custom-call | flops 20971520 | bytes 4194304 | tf_op jit(solution)/shard_map/state_update/pallas_call | solution.py:329
  62.4 1.5 %collective-permute-done.14 = bf16[32,4096]{1,0:T(8,128)(2,1)S(1)} collective-permute-done((bf16[32,4096]{1,0:T(8,128)(2,1)S(1)}, bf16[32,4096]{1,0:T(8,128)(2,1)S(1)}, u32[]{:S(2)}, u32[]{:S(2)}) %collective-permute-start.14) | collective-permute-done | bytes 262176 | tf_op jit(solution)/shard_map/ppermute | solution.py:186
  64.7 0.8 multiply_convert_fusion
  65.5 2.5 %collective-permute-start.17 = (bf16[64,256]{1,0:T(8,128)(2,1)S(1)}, bf16[64,256]{1,0:T(8,128)(2,1)S(1)}, u32[]{:S(2)}, u32[]{:S(2)}) collective-permute-start(bf16[64,256]{1,0:T(8,128)(2,1)S(1)} %multiply_convert_fusion), channel_id=1, source_target_pairs={{0,3},{1,2},{2,1},{3,0},{4,7},{5,6},{6,5},{7,4},{8,11},{9,10},{10,... | collective-permute-start | bytes 98312 | tf_op jit(solution)/shard_map/ppermute | solution.py:186
  69.0 3.8 %state_update.6.refs_4_ = f32[16,128,1024]{2,1,0:T(8,128)} custom-call(f32[16,512]{1,0:T(8,128)S(1)} %fusion.39.refs_5_.refs_0_, f32[16,512]{1,0:T(8,128)S(1)} %get-tuple-element.21.refs_1_, f32[16,1024]{1,0:T(8,128)S(1)} %get-tuple-element.22.refs_2_, f32[16,128,1024]{2,1,0:T(8,128)} %refs_3_.7, ...), custom_call_target="tpu_custom_call", output_to_operand_aliasing={{}: (4, {})} | custom-call | flops 15728640 | bytes 3145728 | tf_op jit(solution)/shard_map/state_update/pallas_call | solution.py:329
  73.5 1.2 %collective-permute-done.18 = bf16[32,1024]{1,0:T(8,128)(2,1)S(1)} collective-permute-done((bf16[32,1024]{1,0:T(8,128)(2,1)S(1)}, bf16[32,1024]{1,0:T(8,128)(2,1)S(1)}, u32[]{:S(2)}, u32[]{:S(2)}) %collective-permute-start.18) | collective-permute-done | bytes 65568 | tf_op jit(solution)/shard_map/ppermute | solution.py:186
  74.8 1.1 %collective-permute-start.19 = (bf16[16,1024]{1,0:T(8,128)(2,1)S(1)}, bf16[16,1024]{1,0:T(8,128)(2,1)S(1)}, u32[]{:S(2)}, u32[]{:S(2)}) collective-permute-start(bf16[16,1024]{1,0:T(8,128)(2,1)S(1)} %pad_maximum_fusion.7), channel_id=1, source_target_pairs={{0,8},{4,12},{8,0},{12,4},{16,24},{20,28},{24,16},{28,20},{1,9},{5... | collective-permute-start | bytes 98312 | tf_op jit(solution)/shard_map/ppermute | solution.py:186
  75.8 1.0 %collective-permute-start.20 = (bf16[16,1024]{1,0:T(8,128)(2,1)S(1)}, bf16[16,1024]{1,0:T(8,128)(2,1)S(1)}, u32[]{:S(2)}, u32[]{:S(2)}) collective-permute-start(bf16[16,1024]{1,0:T(8,128)(2,1)S(1)} %pad_maximum_fusion.8), channel_id=1, source_target_pairs={{0,16},{4,20},{8,24},{12,28},{16,0},{20,4},{24,8},{28,12},{1,17},{... | collective-permute-start | bytes 98312 | tf_op jit(solution)/shard_map/ppermute | solution.py:186
  76.8 2.4 %collective-permute-start.21 = (bf16[16,1024]{1,0:T(8,128)(2,1)S(1)}, bf16[16,1024]{1,0:T(8,128)(2,1)S(1)}, u32[]{:S(2)}, u32[]{:S(2)}) collective-permute-start(bf16[16,1024]{1,0:T(8,128)(2,1)S(1)} %pad_maximum_fusion.9), channel_id=1, source_target_pairs={{0,24},{4,28},{8,16},{12,20},{16,8},{20,12},{24,0},{28,4},{1,25},{... | collective-permute-start | bytes 98312 | tf_op jit(solution)/shard_map/ppermute | solution.py:186
  79.2 4.5 %state_update.7 = f32[16,128,1024]{2,1,0:T(8,128)} custom-call(f32[16,512]{1,0:T(8,128)S(1)} %fusion.39.refs_5_.refs_0_, f32[16,512]{1,0:T(8,128)S(1)} %get-tuple-element.21.refs_1_, f32[16,1024]{1,0:T(8,128)S(1)} %get-tuple-element.22.refs_2_, f32[16,128,1024]{2,1,0:T(8,128)} %refs_3_.7, ...), custom_call_target="tpu_custom_call", output_to_operand_aliasing={{}: (4, {})} | custom-call | flops 20971520 | bytes 4194304 | tf_op jit(solution)/shard_map/state_update/pallas_call | solution.py:329
  83.8 0.9 %add_convert_fusion.1 = bf16[16,1024]{1,0:T(8,128)(2,1)} fusion(bf16[16,4096]{1,0:T(8,128)(2,1)S(1)} %get-tuple-element.35, s32[]{:T(128)S(6)} %select_n.113, f32[16,64]{0,1:T(8,128)S(1)} %bitcast.56, bf16[64,1024]{1,0:T(8,128)(2,1)S(1)} %constant_dynamic-update-slice_fusion.5), kind=kOutput, calls=%fused_computation.40 | convolution fusion | flops 12632064 | bytes 200708 | tf_op jit(solution)/shard_map/dot_general | solution.py:499
  (91 shorter events, 7.8 us)
Async XLA Ops:
  0.6 72.3 %copy-start = (bf16[1,1024,1024]{2,1,0:T(8,128)(2,1)S(1)}, bf16[1,1024,1024]{2,1,0:T(8,128)(2,1)}, u32[]{:S(2)}) copy-start(bf16[1,1024,1024]{2,1,0:T(8,128)(2,1)} %param.34) | copy-start | bytes 6291460
  0.6 18.0 %copy-start.3 = (bf16[512,1024]{1,0:T(8,128)(2,1)S(1)}, bf16[512,1024]{1,0:T(8,128)(2,1)}, u32[]{:S(2)}) copy-start(bf16[512,1024]{1,0:T(8,128)(2,1)} %refs_7_.2) | copy-start | bytes 3145732
  0.7 6.7 %collective-permute-start = (bf16[16,4096]{1,0:T(8,128)(2,1)}, bf16[16,4096]{1,0:T(8,128)(2,1)S(1)}, u32[]{:S(2)}, u32[]{:S(2)}) collective-permute-start(bf16[16,4096]{1,0:T(8,128)(2,1)} %param.19), channel_id=1, source_target_pairs={{0,4},{4,0},{8,12},{12,8},{16,20},{20,16},{24,28},{28,24},{1,5},{5... | collective-permute-start | bytes 393224 | tf_op jit(solution)/shard_map/ppermute | solution.py:186
  5.0 13.6 %copy-start.4 = (bf16[512,1024]{1,0:T(8,128)(2,1)S(1)}, bf16[512,1024]{1,0:T(8,128)(2,1)}, u32[]{:S(2)}) copy-start(bf16[512,1024]{1,0:T(8,128)(2,1)} %refs_8_.2) | copy-start | bytes 3145732
  7.3 12.6 %copy-start.10 = (s32[16,2]{0,1:T(2,128)S(1)}, s32[16,2]{0,1:T(2,128)}, u32[]{:S(2)}) copy-start(s32[16,2]{0,1:T(2,128)} %param.35) | copy-start | bytes 388
  7.4 5.5 %collective-permute-start.1 = (bf16[32,512]{1,0:T(8,128)(2,1)S(1)}, bf16[32,512]{1,0:T(8,128)(2,1)S(1)}, u32[]{:S(2)}, u32[]{:S(2)}) collective-permute-start(bf16[32,512]{1,0:T(8,128)(2,1)S(1)} %pad_maximum_fusion.3), channel_id=1, source_target_pairs={{0,8},{4,12},{8,0},{12,4},{16,24},{20,28},{24,16},{28,20},{1,9},{5... | collective-permute-start | bytes 98312 | tf_op jit(solution)/shard_map/ppermute | solution.py:186
  10.3 5.4 %collective-permute-start.2 = (bf16[32,512]{1,0:T(8,128)(2,1)S(1)}, bf16[32,512]{1,0:T(8,128)(2,1)S(1)}, u32[]{:S(2)}, u32[]{:S(2)}) collective-permute-start(bf16[32,512]{1,0:T(8,128)(2,1)S(1)} %pad_maximum_fusion.4), channel_id=1, source_target_pairs={{0,16},{4,20},{8,24},{12,28},{16,0},{20,4},{24,8},{28,12},{1,17},{... | collective-permute-start | bytes 98312 | tf_op jit(solution)/shard_map/ppermute | solution.py:186
  12.9 5.7 %collective-permute-start.3 = (bf16[32,512]{1,0:T(8,128)(2,1)S(1)}, bf16[32,512]{1,0:T(8,128)(2,1)S(1)}, u32[]{:S(2)}, u32[]{:S(2)}) collective-permute-start(bf16[32,512]{1,0:T(8,128)(2,1)S(1)} %pad_maximum_fusion.5), channel_id=1, source_target_pairs={{0,24},{4,28},{8,16},{12,20},{16,8},{20,12},{24,0},{28,4},{1,25},{... | collective-permute-start | bytes 98312 | tf_op jit(solution)/shard_map/ppermute | solution.py:186
  20.0 6.5 %copy-start.11 = (f32[16,2]{0,1:T(2,128)S(1)}, f32[16,2]{0,1:T(2,128)}, u32[]{:S(2)}) copy-start(f32[16,2]{0,1:T(2,128)} %param.36) | copy-start | bytes 388
  20.0 13.0 %copy-start.5 = (f32[256]{0:T(256)S(1)}, f32[256]{0:T(256)}, u32[]{:S(2)}) copy-start(f32[256]{0:T(256)} %param.29) | copy-start | bytes 3076
  20.0 1.9 %collective-permute-start.4 = (bf16[64,3072]{1,0:T(8,128)(2,1)}, bf16[64,3072]{1,0:T(8,128)(2,1)S(1)}, u32[]{:S(2)}, u32[]{:S(2)}) collective-permute-start(bf16[64,3072]{1,0:T(8,128)(2,1)} %get-tuple-element.18), channel_id=1, source_target_pairs={{0,4},{4,0},{8,12},{12,8},{16,20},{20,16},{24,28},{28,24},{1,5},{5... | collective-permute-start | bytes 1179656 | tf_op jit(solution)/shard_map/ppermute | solution.py:186
  22.0 6.1 %collective-permute-start.5 = (bf16[16,3072]{1,0:T(8,128)(2,1)S(1)}, bf16[16,3072]{1,0:T(8,128)(2,1)S(1)}, u32[]{:S(2)}, u32[]{:S(2)}) collective-permute-start(bf16[16,3072]{1,0:T(8,128)(2,1)S(1)} %get-tuple-element.38), channel_id=1, source_target_pairs={{0,8},{4,12},{8,0},{12,4},{16,24},{20,28},{24,16},{28,20},{1,9},{5... | collective-permute-start | bytes 294920 | tf_op jit(solution)/shard_map/ppermute | solution.py:186
  22.1 10.9 %collective-permute-start.6 = (bf16[16,3072]{1,0:T(8,128)(2,1)S(1)}, bf16[16,3072]{1,0:T(8,128)(2,1)S(1)}, u32[]{:S(2)}, u32[]{:S(2)}) collective-permute-start(bf16[16,3072]{1,0:T(8,128)(2,1)S(1)} %get-tuple-element.37), channel_id=1, source_target_pairs={{0,16},{4,20},{8,24},{12,28},{16,0},{20,4},{24,8},{28,12},{1,17},{... | collective-permute-start | bytes 294920 | tf_op jit(solution)/shard_map/ppermute | solution.py:186
  23.0 10.0 %collective-permute-start.7 = (bf16[16,3072]{1,0:T(8,128)(2,1)S(1)}, bf16[16,3072]{1,0:T(8,128)(2,1)S(1)}, u32[]{:S(2)}, u32[]{:S(2)}) collective-permute-start(bf16[16,3072]{1,0:T(8,128)(2,1)S(1)} %get-tuple-element.36), channel_id=1, source_target_pairs={{0,24},{4,28},{8,16},{12,20},{16,8},{20,12},{24,0},{28,4},{1,25},{... | collective-permute-start | bytes 294920 | tf_op jit(solution)/shard_map/ppermute | solution.py:186
  39.8 7.1 %copy-start.12 = (f32[16]{0:T(128)S(1)}, f32[16]{0:T(128)}, u32[]{:S(2)}) copy-start(f32[16]{0:T(128)} %param.37) | copy-start | bytes 196
  43.4 9.1 %collective-permute-start.10 = (bf16[16,4096]{1,0:T(8,128)(2,1)S(1)}, bf16[16,4096]{1,0:T(8,128)(2,1)S(1)}, u32[]{:S(2)}, u32[]{:S(2)}) collective-permute-start(bf16[16,4096]{1,0:T(8,128)(2,1)S(1)} %get-tuple-element.19), channel_id=1, source_target_pairs={{0,3},{1,2},{2,1},{3,0},{4,7},{5,6},{6,5},{7,4},{8,11},{9,10},{10,... | collective-permute-start | bytes 393224 | tf_op jit(solution)/shard_map/ppermute | solution.py:186
  45.8 6.6 %collective-permute-start.9 = (bf16[16,4096]{1,0:T(8,128)(2,1)S(1)}, bf16[16,4096]{1,0:T(8,128)(2,1)S(1)}, u32[]{:S(2)}, u32[]{:S(2)}) collective-permute-start(bf16[16,4096]{1,0:T(8,128)(2,1)S(1)} %get-tuple-element.19), channel_id=1, source_target_pairs={{0,2},{1,3},{2,0},{3,1},{4,6},{5,7},{6,4},{7,5},{8,10},{9,11},{10,... | collective-permute-start | bytes 393224 | tf_op jit(solution)/shard_map/ppermute | solution.py:186
  46.3 6.1 %collective-permute-start.8 = (bf16[16,4096]{1,0:T(8,128)(2,1)S(1)}, bf16[16,4096]{1,0:T(8,128)(2,1)S(1)}, u32[]{:S(2)}, u32[]{:S(2)}) collective-permute-start(bf16[16,4096]{1,0:T(8,128)(2,1)S(1)} %get-tuple-element.19), channel_id=1, source_target_pairs={{0,1},{1,0},{2,3},{3,2},{4,5},{5,4},{6,7},{7,6},{8,9},{9,8},{10,11... | collective-permute-start | bytes 393224 | tf_op jit(solution)/shard_map/ppermute | solution.py:186
  46.9 5.6 %copy-start.8 = (bf16[16,4096]{1,0:T(8,128)(2,1)S(1)}, bf16[16,4096]{1,0:T(8,128)(2,1)}, u32[]{:S(2)}) copy-start(bf16[16,4096]{1,0:T(8,128)(2,1)} %param.19) | copy-start | bytes 393220
  46.9 5.8 %copy-start.9 = (f32[4096]{0:T(1024)S(1)}, f32[4096]{0:T(1024)}, u32[]{:S(2)}) copy-start(f32[4096]{0:T(1024)} %param.31) | copy-start | bytes 49156
  53.1 9.1 %collective-permute-start.11 = (bf16[8,4096]{1,0:T(8,128)(2,1)S(1)}, bf16[8,4096]{1,0:T(8,128)(2,1)S(1)}, u32[]{:S(2)}, u32[]{:S(2)}) collective-permute-start(bf16[8,4096]{1,0:T(8,128)(2,1)S(1)} %get-tuple-element.44), channel_id=1, source_target_pairs={{0,8},{4,12},{8,0},{12,4},{16,24},{20,28},{24,16},{28,20},{1,9},{5... | collective-permute-start | bytes 196616 | tf_op jit(solution)/shard_map/ppermute | solution.py:186
  55.1 7.2 %collective-permute-start.12 = (bf16[8,4096]{1,0:T(8,128)(2,1)S(1)}, bf16[8,4096]{1,0:T(8,128)(2,1)S(1)}, u32[]{:S(2)}, u32[]{:S(2)}) collective-permute-start(bf16[8,4096]{1,0:T(8,128)(2,1)S(1)} %get-tuple-element.43), channel_id=1, source_target_pairs={{0,16},{4,20},{8,24},{12,28},{16,0},{20,4},{24,8},{28,12},{1,17},{... | collective-permute-start | bytes 196616 | tf_op jit(solution)/shard_map/ppermute | solution.py:186
  55.1 7.1 %collective-permute-start.13 = (bf16[8,4096]{1,0:T(8,128)(2,1)S(1)}, bf16[8,4096]{1,0:T(8,128)(2,1)S(1)}, u32[]{:S(2)}, u32[]{:S(2)}) collective-permute-start(bf16[8,4096]{1,0:T(8,128)(2,1)S(1)} %get-tuple-element.42), channel_id=1, source_target_pairs={{0,24},{4,28},{8,16},{12,20},{16,8},{20,12},{24,0},{28,4},{1,25},{... | collective-permute-start | bytes 196616 | tf_op jit(solution)/shard_map/ppermute | solution.py:186
  57.6 6.3 %copy-start.6 = (bf16[1,256,4096]{2,1,0:T(8,128)(2,1)S(1)}, bf16[1,256,4096]{2,1,0:T(8,128)(2,1)}, u32[]{:S(2)}) copy-start(bf16[1,256,4096]{2,1,0:T(8,128)(2,1)} %param.32) | copy-start | bytes 6291460
  62.3 1.6 %collective-permute-start.14 = (bf16[32,4096]{1,0:T(8,128)(2,1)S(1)}, bf16[32,4096]{1,0:T(8,128)(2,1)S(1)}, u32[]{:S(2)}, u32[]{:S(2)}) collective-permute-start(bf16[32,4096]{1,0:T(8,128)(2,1)S(1)} %pad_maximum_fusion), channel_id=1, source_target_pairs={{0,4},{4,0},{8,12},{12,8},{16,20},{20,16},{24,28},{28,24},{1,5},{5... | collective-permute-start | bytes 786440 | tf_op jit(solution)/shard_map/ppermute | solution.py:186
  65.5 7.4 %collective-permute-start.17 = (bf16[64,256]{1,0:T(8,128)(2,1)S(1)}, bf16[64,256]{1,0:T(8,128)(2,1)S(1)}, u32[]{:S(2)}, u32[]{:S(2)}) collective-permute-start(bf16[64,256]{1,0:T(8,128)(2,1)S(1)} %multiply_convert_fusion), channel_id=1, source_target_pairs={{0,3},{1,2},{2,1},{3,0},{4,7},{5,6},{6,5},{7,4},{8,11},{9,10},{10,... | collective-permute-start | bytes 98312 | tf_op jit(solution)/shard_map/ppermute | solution.py:186
  68.0 4.9 %collective-permute-start.16 = (bf16[64,256]{1,0:T(8,128)(2,1)S(1)}, bf16[64,256]{1,0:T(8,128)(2,1)S(1)}, u32[]{:S(2)}, u32[]{:S(2)}) collective-permute-start(bf16[64,256]{1,0:T(8,128)(2,1)S(1)} %multiply_convert_fusion), channel_id=1, source_target_pairs={{0,2},{1,3},{2,0},{3,1},{4,6},{5,7},{6,4},{7,5},{8,10},{9,11},{10,... | collective-permute-start | bytes 98312 | tf_op jit(solution)/shard_map/ppermute | solution.py:186
  68.5 4.4 %collective-permute-start.15 = (bf16[64,256]{1,0:T(8,128)(2,1)S(1)}, bf16[64,256]{1,0:T(8,128)(2,1)S(1)}, u32[]{:S(2)}, u32[]{:S(2)}) collective-permute-start(bf16[64,256]{1,0:T(8,128)(2,1)S(1)} %multiply_convert_fusion), channel_id=1, source_target_pairs={{0,1},{1,0},{2,3},{3,2},{4,5},{5,4},{6,7},{7,6},{8,9},{9,8},{10,11... | collective-permute-start | bytes 98312 | tf_op jit(solution)/shard_map/ppermute | solution.py:186
  73.4 1.3 %collective-permute-start.18 = (bf16[32,1024]{1,0:T(8,128)(2,1)S(1)}, bf16[32,1024]{1,0:T(8,128)(2,1)S(1)}, u32[]{:S(2)}, u32[]{:S(2)}) collective-permute-start(bf16[32,1024]{1,0:T(8,128)(2,1)S(1)} %slice.77), channel_id=1, source_target_pairs={{0,4},{4,0},{8,12},{12,8},{16,20},{20,16},{24,28},{28,24},{1,5},{5... | collective-permute-start | bytes 196616 | tf_op jit(solution)/shard_map/ppermute | solution.py:186
  74.8 8.9 %collective-permute-start.19 = (bf16[16,1024]{1,0:T(8,128)(2,1)S(1)}, bf16[16,1024]{1,0:T(8,128)(2,1)S(1)}, u32[]{:S(2)}, u32[]{:S(2)}) collective-permute-start(bf16[16,1024]{1,0:T(8,128)(2,1)S(1)} %pad_maximum_fusion.7), channel_id=1, source_target_pairs={{0,8},{4,12},{8,0},{12,4},{16,24},{20,28},{24,16},{28,20},{1,9},{5... | collective-permute-start | bytes 98312 | tf_op jit(solution)/shard_map/ppermute | solution.py:186
  75.8 7.9 %collective-permute-start.20 = (bf16[16,1024]{1,0:T(8,128)(2,1)S(1)}, bf16[16,1024]{1,0:T(8,128)(2,1)S(1)}, u32[]{:S(2)}, u32[]{:S(2)}) collective-permute-start(bf16[16,1024]{1,0:T(8,128)(2,1)S(1)} %pad_maximum_fusion.8), channel_id=1, source_target_pairs={{0,16},{4,20},{8,24},{12,28},{16,0},{20,4},{24,8},{28,12},{1,17},{... | collective-permute-start | bytes 98312 | tf_op jit(solution)/shard_map/ppermute | solution.py:186
  76.8 6.9 %collective-permute-start.21 = (bf16[16,1024]{1,0:T(8,128)(2,1)S(1)}, bf16[16,1024]{1,0:T(8,128)(2,1)S(1)}, u32[]{:S(2)}, u32[]{:S(2)}) collective-permute-start(bf16[16,1024]{1,0:T(8,128)(2,1)S(1)} %pad_maximum_fusion.9), channel_id=1, source_target_pairs={{0,24},{4,28},{8,16},{12,20},{16,8},{20,12},{24,0},{28,4},{1,25},{... | collective-permute-start | bytes 98312 | tf_op jit(solution)/shard_map/ppermute | solution.py:186
  (3 other events, 9.2 us)
